TPU v7x, 512 devices: a whole 4x4x16 slice. The times are simulated.
512 devices in a mesh: dp: 4 (over x), kv: 64 (over z, y), tp: 2 (over core).
Axes of the slice: x: 4, y: 4, z: 16, core: 2. Of those that a mesh axis runs over, the one named last changes fastest.
Arguments:
- residual: bfloat16 [32, 2048], P('dp', ('kv', 'tp')), may hold values from -6 to 6
- norm_gains: float32 [3, 2048], replicated, may hold values from 0.1 to 1.9
- ffn_gate: bfloat16 [2, 5632, 2048], P(None, ('kv', 'tp')), may hold values from -0.125 to 0.125
- ffn_up: bfloat16 [2, 5632, 2048], P(None, ('kv', 'tp')), may hold values from -0.125 to 0.125
- ffn_down: bfloat16 [2, 5632, 2048], P(None, ('kv', 'tp')), may hold values from -0.1875 to 0.1875
- proj_query: bfloat16 [2048, 1024], P('kv', 'tp'), may hold values from -0.44194174 to 0.44194174
- proj_key: bfloat16 [2048, 256], P('kv', 'tp'), may hold values from -0.125 to 0.125
- proj_value: bfloat16 [2048, 256], P('kv', 'tp'), may hold values from -0.125 to 0.125
- proj_out: bfloat16 [1024, 2048], P('tp', 'kv'), may hold values from -0.1875 to 0.1875
- head_lambda: float32 [8], P('tp'), may hold values from 0.3 to 0.8
- head_gain: float32 [128], replicated, may hold values from 0.1 to 1.9
- cache_keys: bfloat16 [32, 16384, 2, 128], P('dp', 'kv', 'tp'), may hold values from -12 to 12
- cache_values: bfloat16 [32, 16384, 2, 128], P('dp', 'kv', 'tp'), may hold values from -6 to 6
- live_length: int32 [32], P('dp'), may hold values from 1 to 16384, 131072 in all
Outputs:
- updated: bfloat16 [32, 2048], P('dp', ('kv', 'tp'))
Inputs may be any that keep to these rules, and one draw needn't show every extreme that they name: `live_length`: the largest length of every draw equals 16384.
All inputs are finite; a program needn't handle non-finite values. No bound on the sum of `live_length` on one device may be relied on, other than what follows from the above.
Results may differ from a plain program's by a relative error of at most 0.014.
The roundings to bfloat16 on the way count: a program that leaves them out, or rounds other values in their place, can miss the bound.
Values may be sent and summed in bfloat16 or wider, within the bound.
A program may use at most 64 MiB of HBM per device.

v0:
```python
import jax
import jax.numpy as jnp
from jax import lax
from jax.sharding import Mesh
from jax.sharding import PartitionSpec as P

D = 2048
HEAD = 64
VDIM = 128
KV_TP = ("kv_0", "kv_1", "tp")
KV = ("kv_0", "kv_1")


epsilon = 1e-05


def sent_to_all(value, axis):
    devices = lax.axis_size(axis)
    return lax.all_to_all(
        jnp.broadcast_to(value[None], (devices, *value.shape)), axis, 0, 0, tiled=True
    )


def in_order(blocks, dim):
    blocks = jnp.moveaxis(blocks, 0, dim)
    shape = blocks.shape
    return blocks.reshape(*shape[:dim], shape[dim] * shape[dim + 1], *shape[dim + 2 :])


def gather_axes(value, axes, dim):
    far, near = axes
    first = sent_to_all(value, far)
    blocks = jnp.swapaxes(sent_to_all(first, near), 0, 1)
    return in_order(blocks.reshape(-1, *value.shape), dim)


def cut_along(value, dim, devices):
    shape = value.shape
    blocks = value.reshape(*shape[:dim], devices, shape[dim] // devices, *shape[dim + 1 :])
    return jnp.moveaxis(blocks, dim, 0)


def sent_and_summed(value, axis, dim):
    devices = lax.axis_size(axis)
    blocks = lax.all_to_all(cut_along(value, dim, devices), axis, 0, 0, tiled=True)
    return jnp.sum(blocks, axis=0)


def summed_rows(value, axes, dim):
    far, near = axes
    blocks = cut_along(value, dim, lax.axis_size(far))
    nearer = sent_and_summed(blocks, near, dim + 1)
    arrived = lax.all_to_all(nearer, far, split_axis=0, concat_axis=0, tiled=True)
    return arrived.sum(axis=0)


def filled_up(lines, devices):
    spare = -len(lines) % devices
    return jnp.pad(lines, [(0, spare)] + [(0, 0)] * (lines.ndim - 1))


def sum_by_parts(value, axes):
    lines = value.reshape(-1)
    own = summed_rows(filled_up(lines, lax.axis_size(axes[0]) * lax.axis_size(axes[1])), axes, 0)
    whole = gather_axes(own, axes, 0)
    return whole[: len(lines)].reshape(value.shape)


def by_axis(value, axes):
    for axis in axes:
        value = lax.psum(value, axis)
    return value


def all_in_one(value, axis):
    leaves = jax.tree.leaves(value)
    order = sorted(range(len(leaves)), key=lambda k: -leaves[k].size)
    width = (1, *leaves[order[0]].shape)[-1]
    lines = [
        jnp.pad(leaves[k].reshape(-1), (0, -leaves[k].size % width)).reshape(-1, width)
        for k in order
    ]
    both, at, found = (lax.all_gather(jnp.concatenate(lines), axis), 0, {})
    for k, line in zip(order, lines):
        piece = both[:, at : at + len(line)].reshape(len(both), -1)
        found[k] = piece[:, : leaves[k].size].reshape(-1, *leaves[k].shape)
        at += len(line)
    numbers = iter(range(len(leaves)))
    return jax.tree.map(lambda _: found[next(numbers)], value)


def merged_by_axis(value, axes, combine):
    for axis in axes:
        pieces = all_in_one(value, axis)
        value = jax.tree.map(lambda part: part[0], pieces)
        for k in range(1, lax.axis_size(axis)):
            value = combine(value, jax.tree.map(lambda part: part[k], pieces))
    return value


def row_scale(row_data):
    data32 = row_data.astype(jnp.float32)
    return lax.rsqrt(jnp.mean(data32 * data32, axis=-1, keepdims=True) + epsilon)


def channel_mix(row_data, gain, gate_part, up_part, down_part):
    normed = (row_data.astype(jnp.float32) * row_scale(row_data) * gain).astype(jnp.bfloat16)
    contract = (((1,), (1,)), ((), ()))
    gate_act = lax.dot_general(normed, gate_part, contract, preferred_element_type=jnp.float32)
    up_act = lax.dot_general(normed, up_part, contract, preferred_element_type=jnp.float32)
    hidden = (jax.nn.silu(gate_act) * up_act).astype(jnp.bfloat16)
    return 0.5 * jnp.dot(hidden, down_part, preferred_element_type=jnp.float32)


def join_parts(earlier, latter):
    highest = jnp.maximum(earlier[0], latter[0])
    weight_early = jnp.exp(earlier[0] - highest)
    weight_late = jnp.exp(latter[0] - highest)
    return (
        highest,
        earlier[1] * weight_early + latter[1] * weight_late,
        earlier[2] * weight_early[..., None] + latter[2] * weight_late[..., None],
    )


def local(
    residual,
    norm_gains,
    ffn_gate,
    ffn_up,
    ffn_down,
    proj_query,
    proj_key,
    proj_value,
    proj_out,
    head_lambda,
    head_gain,
    cache_keys,
    cache_values,
    live_length,
):
    rows_one = gather_axes(residual, (("kv_0", "kv_1"), "tp"), 1)
    term_one = channel_mix(rows_one, norm_gains[0], ffn_gate[0], ffn_up[0], ffn_down[0])
    kv_place = lax.axis_index(KV)
    block_width = proj_query.shape[0]
    own_width = residual.shape[1]
    summed = sum_by_parts(term_one, (("kv_0", "kv_1"), "tp"))
    stream_rows = (rows_one.astype(jnp.float32) + summed).astype(jnp.bfloat16)
    row_block = lax.dynamic_slice_in_dim(stream_rows, kv_place * block_width, block_width, 1)
    column_start = (kv_place * lax.axis_size("tp") + lax.axis_index("tp")) * own_width
    stream_own = lax.dynamic_slice_in_dim(stream_rows, column_start, own_width, 1)
    gain_block = lax.dynamic_slice_in_dim(norm_gains[1], kv_place * block_width, block_width, 0)
    block_data = row_block.astype(jnp.float32)
    squares = jnp.sum(block_data * block_data, axis=1)
    scaled = (block_data * gain_block).astype(jnp.bfloat16)
    query_part = jnp.dot(scaled, proj_query, preferred_element_type=jnp.float32)
    key_part = jnp.dot(scaled, proj_key, preferred_element_type=jnp.float32)
    value_part = jnp.dot(scaled, proj_value, preferred_element_type=jnp.float32)
    queries, key_new, value_new, square_sum = (
        by_axis(query_part, KV),
        by_axis(key_part, KV),
        by_axis(value_part, KV),
        by_axis(squares, KV),
    )
    factor = lax.rsqrt(square_sum / D + epsilon)[:, None]
    batch_rows = residual.shape[0]
    kv_local = key_new.shape[1] // (2 * HEAD)
    group_size = queries.shape[1] // (2 * HEAD * kv_local)
    queries = (
        (queries * factor).astype(jnp.bfloat16).reshape(batch_rows, kv_local, group_size, 2, HEAD)
    )
    key_new = (key_new * factor).astype(jnp.bfloat16).reshape(batch_rows, kv_local, 2, HEAD)
    value_new = (value_new * factor).astype(jnp.bfloat16).reshape(batch_rows, kv_local, VDIM)
    span = cache_keys.shape[1]
    block_keys = cache_keys.reshape(batch_rows, span, kv_local, 2, HEAD)
    score_scale = HEAD ** (-0.5)
    scores = (
        jnp.einsum("bkgcd,bpkcd->bkgcp", queries, block_keys, preferred_element_type=jnp.float32)
        * score_scale
    )
    positions = kv_place * span + jnp.arange(span, dtype=jnp.int32)
    live_mask = (positions[None, :] < live_length[:, None])[:, None, None, None, :]
    highest = jnp.max(jnp.where(live_mask, scores, -1e30), axis=-1)
    exp_terms = jnp.where(live_mask, jnp.exp(scores - highest[..., None]), 0.0)
    totals = jnp.sum(exp_terms, axis=-1)
    weights = exp_terms.astype(jnp.bfloat16)
    partial_value = jnp.einsum(
        "bkgcp,bpkv->bkgcv", weights, cache_values, preferred_element_type=jnp.float32
    )
    running = merged_by_axis((highest, totals, partial_value), KV, join_parts)
    lead_shape = totals.shape
    own_scores = (
        jnp.einsum("bkgcd,bkcd->bkgc", queries, key_new, preferred_element_type=jnp.float32)
        * score_scale
    )
    own_values = jnp.broadcast_to(
        value_new.astype(jnp.float32)[:, :, None, None, :], lead_shape + (VDIM,)
    )
    highest, totals, accum = join_parts(
        running, (own_scores, jnp.ones(lead_shape, jnp.float32), own_values)
    )
    ratios = accum / totals[..., None]
    lambdas = head_lambda.reshape(kv_local, group_size)
    mixed_heads = ratios[:, :, :, 0] - lambdas[None, :, :, None] * ratios[:, :, :, 1]
    heads_out = (mixed_heads * row_scale(mixed_heads) * head_gain).astype(jnp.bfloat16)
    heads_out = heads_out.reshape(batch_rows, kv_local * group_size * VDIM)
    out_part = jnp.dot(heads_out, proj_out, preferred_element_type=jnp.float32)
    mixer_out = sent_and_summed(out_part, "tp", 1)
    stream_two = (stream_own.astype(jnp.float32) + mixer_out).astype(jnp.bfloat16)
    rows_two = gather_axes(stream_two, (("kv_0", "kv_1"), "tp"), 1)
    term_two = channel_mix(rows_two, norm_gains[2], ffn_gate[1], ffn_up[1], ffn_down[1])
    summed_two = summed_rows(term_two, (("kv_0", "kv_1"), "tp"), 1)
    return (stream_two.astype(jnp.float32) + summed_two).astype(jnp.bfloat16)


def solution(mesh):
    split = Mesh(
        mesh.devices.reshape(mesh.shape["dp"], 16, 4, mesh.shape["tp"]),
        ("dp", "kv_0", "kv_1", "tp"),
    )
    return jax.shard_map(
        local,
        mesh=split,
        in_specs=(
            P("dp", KV_TP),
            P(),
            P(None, KV_TP, None),
            P(None, KV_TP, None),
            P(None, KV_TP, None),
            P(KV, "tp"),
            P(KV, "tp"),
            P(KV, "tp"),
            P("tp", KV),
            P("tp"),
            P(),
            P("dp", KV, "tp", None),
            P("dp", KV, "tp", None),
            P("dp"),
        ),
        out_specs=P("dp", KV_TP),
        check_vma=False,
    )
```

profile of v0, /device:TPU:1, one launch (start us, length us, event | category | flops | bytes accessed | tf_op | source)
XLA Modules:
  0.0 272.4 jit_solution(7751740168058002189)
XLA Ops:
  0.0 1.4 broadcast_in_dim.34
  1.4 19.3 %all-to-all-start = ((bf16[64,8,16]{2,1,0:T(8,128)(2,1)}), bf16[64,8,16]{2,1,0:T(8,128)(2,1)S(1)}, u32[]{:S(2)}, u32[]{:S(2)}) async-start(bf16[64,8,16]{2,1,0:T(8,128)(2,1)} %broadcast_in_dim.34), calls=%async_computation | async-start | bytes 262144 | tf_op jit(solution)/shard_map/all_to_all | solution.py:19
  20.7 0.5 fusion.163
  21.2 0.5 copy-done.2
  21.7 0.5 fusion.164
  22.2 0.5 copy-done.3
  22.7 0.5 fusion.165
  23.2 0.3 copy-done.7
  23.6 12.2 %all-to-all-done = bf16[64,8,16]{2,1,0:T(8,128)(2,1)S(1)} async-done(((bf16[64,8,16]{2,1,0:T(8,128)(2,1)}), bf16[64,8,16]{2,1,0:T(8,128)(2,1)S(1)}, u32[]{:S(2)}, u32[]{:S(2)}) %all-to-all-start) | async-done | bytes 16416 | tf_op jit(solution)/shard_map/all_to_all | solution.py:19
  36.0 7.0 %all_to_all.60 = bf16[2,2,4096]{2,1,0:T(2,128)(2,1)S(1)} all-to-all(bf16[2,2,4096]{2,1,0:T(2,128)(2,1)S(1)} %reshape.2777), channel_id=1, replica_groups=mesh['dp'=4,'kv_0'=16,'kv_1'=4,'tp'=2] {'tp'}, dimensions={0} | all-to-all | bytes 65536 | tf_op jit(solution)/shard_map/all_to_all | solution.py:19
  43.1 0.3 copy.136
  43.4 0.2 fusion.10
  43.9 0.3 convert_element_type.123
  44.4 0.4 convolution_multiply_fusion.1
  44.9 3.9 %all_to_all.61 = f32[2,64,128]{2,1,0:T(8,128)S(1)} all-to-all(f32[2,64,128]{2,1,0:T(8,128)S(1)} %bitcast.691), channel_id=1, replica_groups=mesh['dp'=4,'kv_0'=16,'kv_1'=4,'tp'=2] {'tp'}, dimensions={0} | all-to-all | bytes 131072 | tf_op jit(solution)/shard_map/all_to_all | solution.py:45
  48.8 0.6 reduce_sum.91
  49.4 4.6 %all-to-all-start.3 = ((f32[64,1,128]{2,1,0:T(1,128)}), f32[64,1,128]{2,1,0:T(1,128)S(1)}, u32[]{:S(2)}, u32[]{:S(2)}) async-start(f32[64,1,128]{2,1,0:T(1,128)} %bitcast.8), calls=%async_computation.3 | async-start | bytes 65536 | tf_op jit(solution)/shard_map/all_to_all | solution.py:53
  54.1 13.4 %all-to-all-done.3 = f32[64,1,128]{2,1,0:T(1,128)S(1)} async-done(((f32[64,1,128]{2,1,0:T(1,128)}), f32[64,1,128]{2,1,0:T(1,128)S(1)}, u32[]{:S(2)}, u32[]{:S(2)}) %all-to-all-start.3) | async-done | bytes 32800 | tf_op jit(solution)/shard_map/all_to_all | solution.py:53
  67.5 0.6 broadcast_in_dim.36
  68.2 4.7 %all-to-all-start.4 = ((f32[64,1,128]{2,1,0:T(1,128)}), f32[64,1,128]{2,1,0:T(1,128)S(1)}, u32[]{:S(2)}, u32[]{:S(2)}) async-start(f32[64,1,128]{2,1,0:T(1,128)} %broadcast_in_dim.36), calls=%async_computation.4 | async-start | bytes 65536 | tf_op jit(solution)/shard_map/all_to_all | solution.py:19
  73.4 0.3 reshape.2694
  73.7 12.7 %all-to-all-done.4 = f32[64,1,128]{2,1,0:T(1,128)S(1)} async-done(((f32[64,1,128]{2,1,0:T(1,128)}), f32[64,1,128]{2,1,0:T(1,128)S(1)}, u32[]{:S(2)}, u32[]{:S(2)}) %all-to-all-start.4) | async-done | bytes 32800 | tf_op jit(solution)/shard_map/all_to_all | solution.py:19
  86.4 6.4 %all_to_all.62 = f32[2,64,128]{2,1,0:T(8,128)S(1)} all-to-all(f32[2,64,128]{2,1,0:T(8,128)S(1)} %broadcast_in_dim.38), channel_id=1, replica_groups=mesh['dp'=4,'kv_0'=16,'kv_1'=4,'tp'=2] {'tp'}, dimensions={0} | all-to-all | bytes 131072 | tf_op jit(solution)/shard_map/all_to_all | solution.py:19
  93.2 0.5 copy-done.8
  94.2 38.9 %all-reduce.4 = (f32[8,512]{1,0:T(8,128)S(1)}, f32[8]{0:T(128)S(1)}, f32[8,128]{1,0:T(8,128)S(1)}, f32[8,128]{1,0:T(8,128)S(1)}) all-reduce(f32[8,512]{1,0:T(8,128)S(1)} %fusion.151, f32[8]{0:T(128)S(1)} %fusion.68, f32[8,128]{1,0:T(8,128)S(1)} %fusion.149, ...), channel_id=1, replica_groups=mesh['dp'=4,'kv_0'=16,'kv_1'=4,'tp'=2] {'kv_0'}, use_global_device_ids=true, to_apply=%region_3.4 | all-reduce | flops 6152 | bytes 49216 | tf_op jit(solution)/shard_map/psum | solution.py:71
  133.1 12.4 %all-reduce.5 = (f32[8,512]{1,0:T(8,128)S(1)}, f32[8]{0:T(128)S(1)}, f32[8,128]{1,0:T(8,128)S(1)}, f32[8,128]{1,0:T(8,128)S(1)}) all-reduce(f32[8,512]{1,0:T(8,128)S(1)} %get-tuple-element.15, f32[8]{0:T(128)S(1)} %get-tuple-element.16, ...), channel_id=1, replica_groups=mesh['dp'=4,'kv_0'=16,'kv_1'=4,'tp'=2] {'kv_1'}, use_global_device_ids=true, to_apply=%region_4.5 | all-reduce | flops 6152 | bytes 49216 | tf_op jit(solution)/shard_map/psum | solution.py:71
  145.7 0.3 select_reduce_fusion
  146.9 22.2 %all-gather.2 = f32[16,66,128]{2,1,0:T(8,128)S(1)} all-gather(f32[1,66,128]{2,1,0:T(8,128)S(1)} %maximum_bitcast_fusion), channel_id=2, replica_groups=mesh['dp'=4,'kv_0'=16,'kv_1'=4,'tp'=2] {'kv_0'}, dimensions={0}, use_global_device_ids=true | all-gather | bytes 574464 | tf_op jit(solution)/shard_map/all_gather | solution.py:83
  169.2 0.3 fusion.17
  169.6 9.3 %all-gather.3 = f32[4,66,128]{2,1,0:T(8,128)S(1)} all-gather(f32[1,66,128]{2,1,0:T(8,128)S(1)} %maximum_bitcast_fusion.1), channel_id=3, replica_groups=mesh['dp'=4,'kv_0'=16,'kv_1'=4,'tp'=2] {'kv_1'}, dimensions={0}, use_global_device_ids=true | all-gather | bytes 168960 | tf_op jit(solution)/shard_map/all_gather | solution.py:83
  182.1 0.4 add_divide_fusion
  182.6 0.6 copy-done.10
  183.5 0.6 copy-done.5
  184.3 30.5 %all_to_all.63 = f32[2,1,128]{2,1,0:T(1,128)S(1)} all-to-all(f32[2,1,128]{2,1,0:T(1,128)S(1)} %reshape.2779), channel_id=1, replica_groups=mesh['dp'=4,'kv_0'=16,'kv_1'=4,'tp'=2] {'tp'}, dimensions={0} | all-to-all | bytes 2048 | tf_op jit(solution)/shard_map/all_to_all | solution.py:45
  214.8 0.5 broadcast.484
  215.3 0.7 reduce.56
  216.2 0.7 broadcast_in_dim.43
  216.8 7.3 %all-to-all-start.7 = ((bf16[64,8,16]{2,1,0:T(8,128)(2,1)}), bf16[64,8,16]{2,1,0:T(8,128)(2,1)S(1)}, u32[]{:S(2)}, u32[]{:S(2)}) async-start(bf16[64,8,16]{2,1,0:T(8,128)(2,1)} %broadcast_in_dim.43), calls=%async_computation.7 | async-start | bytes 262144 | tf_op jit(solution)/shard_map/all_to_all | solution.py:19
  224.2 15.0 %all-to-all-done.7 = bf16[64,8,16]{2,1,0:T(8,128)(2,1)S(1)} async-done(((bf16[64,8,16]{2,1,0:T(8,128)(2,1)}), bf16[64,8,16]{2,1,0:T(8,128)(2,1)S(1)}, u32[]{:S(2)}, u32[]{:S(2)}) %all-to-all-start.7) | async-done | bytes 16416 | tf_op jit(solution)/shard_map/all_to_all | solution.py:19
  239.4 6.8 %all_to_all.64 = bf16[2,2,4096]{2,1,0:T(2,128)(2,1)S(1)} all-to-all(bf16[2,2,4096]{2,1,0:T(2,128)(2,1)S(1)} %reshape.2781), channel_id=1, replica_groups=mesh['dp'=4,'kv_0'=16,'kv_1'=4,'tp'=2] {'tp'}, dimensions={0} | all-to-all | bytes 65536 | tf_op jit(solution)/shard_map/all_to_all | solution.py:19
  246.3 0.3 copy.166
  247.1 0.3 convert_element_type.143
  247.6 0.4 convolution_multiply_fusion
  248.4 3.8 %all_to_all.65 = f32[2,1,8192]{2,1,0:T(1,128)S(1)} all-to-all(f32[2,1,8192]{2,1,0:T(1,128)S(1)} %reshape.2783), channel_id=1, replica_groups=mesh['dp'=4,'kv_0'=16,'kv_1'=4,'tp'=2] {'tp'}, dimensions={0} | all-to-all | bytes 131072 | tf_op jit(solution)/shard_map/all_to_all | solution.py:45
  252.2 0.8 reduce.57
  253.5 17.4 %all_to_all.66 = f32[64,1,128]{2,1,0:T(1,128)S(1)} all-to-all(f32[64,1,128]{2,1,0:T(1,128)S(1)} %reshape.2785), channel_id=1, replica_groups=mesh['dp'=4,'kv_0'=16,'kv_1'=4,'tp'=2] {'kv_0','kv_1'}, dimensions={0} | all-to-all | bytes 65536 | tf_op jit(solution)/shard_map/all_to_all | solution.py:53
  270.9 0.7 reduce.58
  271.8 0.6 add_convert_fusion.1
  (129 shorter events, 9.5 us)
Async XLA Ops:
  0.0 146.7 %copy-start = (bf16[8,256,1,128]{3,1,2,0:T(8,128)(2,1)S(1)}, bf16[8,256,1,128]{3,1,2,0:T(8,128)(2,1)}, u32[]{:S(2)}) copy-start(bf16[8,256,1,128]{3,1,2,0:T(8,128)(2,1)} %param.26) | copy-start | bytes 1572868
  0.0 20.7 %copy-start.1 = (bf16[2,44,2048]{2,0,1:T(2,128)(2,1)S(1)}, bf16[2,44,2048]{2,0,1:T(2,128)(2,1)}, u32[]{:S(2)}) copy-start(bf16[2,44,2048]{2,0,1:T(2,128)(2,1)} %param.16) | copy-start | bytes 1081348
  1.4 34.3 %all-to-all-start = ((bf16[64,8,16]{2,1,0:T(8,128)(2,1)}), bf16[64,8,16]{2,1,0:T(8,128)(2,1)S(1)}, u32[]{:S(2)}, u32[]{:S(2)}) async-start(bf16[64,8,16]{2,1,0:T(8,128)(2,1)} %broadcast_in_dim.34), calls=%async_computation | async-start | bytes 262144 | tf_op jit(solution)/shard_map/all_to_all | solution.py:19
  20.7 1.0 copy-start.2
  21.7 1.0 copy-start.3
  22.7 0.8 copy-start.7
  44.8 28.2 %copy-start.4 = (bf16[8,256,1,128]{3,1,2,0:T(8,128)(2,1)S(1)}, bf16[8,256,1,128]{3,1,2,0:T(8,128)(2,1)}, u32[]{:S(2)}) copy-start(bf16[8,256,1,128]{3,1,2,0:T(8,128)(2,1)} %param.25) | copy-start | bytes 1572868
  49.4 18.1 %all-to-all-start.3 = ((f32[64,1,128]{2,1,0:T(1,128)}), f32[64,1,128]{2,1,0:T(1,128)S(1)}, u32[]{:S(2)}, u32[]{:S(2)}) async-start(f32[64,1,128]{2,1,0:T(1,128)} %bitcast.8), calls=%async_computation.3 | async-start | bytes 65536 | tf_op jit(solution)/shard_map/all_to_all | solution.py:53
  68.2 4.8 %copy-start.12 = (s32[8]{0:T(128)S(1)}, s32[8]{0:T(128)}, u32[]{:S(2)}) copy-start(s32[8]{0:T(128)} %param.27) | copy-start | bytes 100
  68.2 18.2 %all-to-all-start.4 = ((f32[64,1,128]{2,1,0:T(1,128)}), f32[64,1,128]{2,1,0:T(1,128)S(1)}, u32[]{:S(2)}, u32[]{:S(2)}) async-start(f32[64,1,128]{2,1,0:T(1,128)} %broadcast_in_dim.36), calls=%async_computation.4 | async-start | bytes 65536 | tf_op jit(solution)/shard_map/all_to_all | solution.py:19
  92.9 0.7 copy-start.8
  92.9 0.9 copy-start.9
  93.0 1.0 copy-start.6
  182.1 1.3 copy-start.11
  182.5 0.7 copy-start.10
  183.4 0.8 copy-start.5
  216.8 22.3 %all-to-all-start.7 = ((bf16[64,8,16]{2,1,0:T(8,128)(2,1)}), bf16[64,8,16]{2,1,0:T(8,128)(2,1)S(1)}, u32[]{:S(2)}, u32[]{:S(2)}) async-start(bf16[64,8,16]{2,1,0:T(8,128)(2,1)} %broadcast_in_dim.43), calls=%async_computation.7 | async-start | bytes 262144 | tf_op jit(solution)/shard_map/all_to_all | solution.py:19
where the time goes:
time: 273 us; the launch traced here: 272 us
  blocking collectives  159 us (58%)
  waiting for transfers between devices  53.2 us (19%)
  starting transfers between devices  35.9 us (13%)
  local copies, waits for them, and re-layouts  15.3 us (6%)
  other arithmetic  6.24 us (2%)
    psum x2, blocking collectives, by_axis(): value = lax.psum(value, axis)  51.3 us
    all_to_all x3, waiting for transfers between devices, sent_to_all(): lax.all_to_all(jnp.broadcast_to(value[None], (devices, *value.shape)), ax...  39.8 us
    all_to_all x3, blocking collectives, sent_and_summed(): lax.all_to_all(cut_along(value, dim, devices), axis, 0, 0, tiled=True)  38.2 us
    all_gather x2, blocking collectives, all_in_one(): both, at, found = (lax.all_gather(jnp.concatenate(lines), axis), 0, {})  31.5 us
    all_to_all x3, starting transfers between devices, sent_to_all(): lax.all_to_all(jnp.broadcast_to(value[None], (devices, *value.shape)), ax...  31.3 us
    all_to_all x3, blocking collectives, sent_to_all(): lax.all_to_all(jnp.broadcast_to(value[None], (devices, *value.shape)), ax...  20.2 us
    all_to_all x1, blocking collectives, summed_rows(): lax.all_to_all(nearer, far, split_axis=0, concat_axis=0, tiled=True)  17.4 us
    all_to_all x1, waiting for transfers between devices, summed_rows(): lax.all_to_all(nearer, far, split_axis=0, concat_axis=0, tiled=True)  13.4 us
  transfers between devices with their start and end apart: 4, of which 4 were waited for; matrix products, arithmetic and copies ran while one was open for 1% of the time, Pallas kernels for 0%

commit v1 on v0

v1 whole, which is shorter than its diff:
```python
import functools

import jax
import jax.numpy as jnp
from jax import lax
from jax.experimental import pallas as pl
from jax.experimental.pallas import tpu as pltpu
from jax.sharding import Mesh
from jax.sharding import PartitionSpec as P

D = 2048
HEAD = 64
VDIM = 128
NZ = 16
NY = 4
NC = 2
NYC = NY * NC
LANES = 128
KV_TP = ("kv_0", "kv_1", "tp")
KV = ("kv_0", "kv_1")
MESH = pl.DeviceIdType.MESH
F32 = jnp.float32
BF16 = jnp.bfloat16
EPS = 1e-05
NT = (((1,), (1,)), ((), ()))

Z_STEPS = (8, 7, 9, 6, 10, 5, 11, 4, 12, 3, 13, 2, 14, 1, 15)
Y_STEPS = (2, 1, 3)
YC_STEPS = (4, 5, 2, 3, 6, 7, 1)

A1, A2, B1, B2, C1, C2, C3, D1, D2O, D2M, D3, F1, F2, G1, G2 = range(15)


def iota(shape, dim):
    return lax.broadcasted_iota(jnp.int32, shape, dim)


def mix_part(rows, gain, gate_w, up_w, down_w):
    scale = lax.rsqrt(jnp.mean(rows * rows, axis=1, keepdims=True) + EPS)
    normed = (rows * scale * gain).astype(BF16)
    gate = lax.dot_general(normed, gate_w, NT, preferred_element_type=F32)
    up = lax.dot_general(normed, up_w, NT, preferred_element_type=F32)
    hidden = (gate / (1.0 + jnp.exp(-gate)) * up).astype(BF16)
    return 0.5 * jnp.dot(hidden, down_w, preferred_element_type=F32)


def layer_kernel(
    res, gains, gate0, up0, down0, gate1, up1, down1, wq_h, wk_h, wv_h, po_h, lam, hgain, ck_h, cv_h, live,
    out,
    wst, po, kbuf, vbuf, wpl, popl,
    a1, a2, b1s, b1r, b2, c1s, c1r, c2, c3, d1s, d1r, d2o, d2m, d3, f1, f2, g1s, g1r, g2,
    hsem, ssem, rsem,
):
    z = lax.axis_index("kv_0")
    y = lax.axis_index("kv_1")
    c = lax.axis_index("tp")
    yc = y * NC + c

    loads = [
        pltpu.make_async_copy(wq_h, wst.at[:, pl.ds(0, 512)], hsem.at[0]),
        pltpu.make_async_copy(wk_h, wst.at[:, pl.ds(512, 128)], hsem.at[1]),
        pltpu.make_async_copy(wv_h, wst.at[:, pl.ds(640, 128)], hsem.at[2]),
        pltpu.make_async_copy(po_h, po, hsem.at[3]),
        pltpu.make_async_copy(ck_h, kbuf, hsem.at[4]),
        pltpu.make_async_copy(cv_h, vbuf, hsem.at[5]),
    ]
    for load in loads:
        load.start()

    def z_peer(k):
        return lax.rem(z + k, NZ)

    def y_peer(k):
        return lax.rem(y + k, NY)

    def yc_peer(k):
        p = lax.rem(yc + k, NYC)
        return p // NC, lax.rem(p, NC)

    barrier = pltpu.get_barrier_semaphore()
    for k in Z_STEPS:
        pl.semaphore_signal(barrier, inc=1, device_id={"kv_0": z_peer(k)}, device_id_type=MESH)
    for k in YC_STEPS:
        py, pc = yc_peer(k)
        pl.semaphore_signal(barrier, inc=1, device_id={"kv_1": py, "tp": pc}, device_id_type=MESH)

    sent = []

    def send(phase, src, dst, device):
        pltpu.make_async_remote_copy(
            src_ref=src, dst_ref=dst, send_sem=ssem.at[phase], recv_sem=rsem.at[phase],
            device_id=device, device_id_type=MESH,
        ).start()

    def arrive(phase, buf, count):
        whole = pltpu.make_async_remote_copy(
            src_ref=buf.at[pl.ds(0, count)], dst_ref=buf.at[pl.ds(0, count)],
            send_sem=ssem.at[phase], recv_sem=rsem.at[phase],
            device_id={"kv_0": z}, device_id_type=MESH,
        )
        whole.wait_recv()
        sent.append(whole)

    def to_z(phase, buf):
        for k in Z_STEPS:
            send(phase, buf.at[z], buf.at[z], {"kv_0": z_peer(k)})

    def to_yc(phase, buf):
        for k in YC_STEPS:
            py, pc = yc_peer(k)
            send(phase, buf.at[yc], buf.at[yc], {"kv_1": py, "tp": pc})

    def to_y(phase, buf):
        for k in Y_STEPS:
            send(phase, buf.at[y], buf.at[y], {"kv_1": y_peer(k)})

    def parts_to_z(phase, src, dst):
        for k in Z_STEPS:
            p = z_peer(k)
            send(phase, src.at[p], dst.at[z], {"kv_0": p})

    def total(buf, count):
        acc = buf[0].astype(F32)
        for k in range(1, count):
            acc = acc + buf[k].astype(F32)
        return acc

    own_lane = yc * 16
    spread = (iota((16, LANES), 1) == iota((16, LANES), 0) + own_lane).astype(F32).astype(BF16)
    a1[yc] = jnp.dot(res[...], spread, preferred_element_type=F32).astype(BF16)
    chip_rows = (iota((LANES, 32), 0) == iota((LANES, 32), 1) + y * 32).astype(F32).astype(BF16)
    for load in loads[:4]:
        load.wait()
    wpl[...] = jnp.dot(chip_rows, wst[...], preferred_element_type=F32).astype(BF16)
    popl[...] = jnp.dot(chip_rows, po[...], preferred_element_type=F32).astype(BF16)

    pl.semaphore_wait(barrier, len(Z_STEPS) + len(YC_STEPS))

    to_yc(A1, a1)
    arrive(A1, a1, NYC - 1)
    res_z = total(a1, NYC)
    a2[z] = res_z.astype(BF16)
    to_z(A2, a2)
    arrive(A2, a2, NZ - 1)
    rows = jnp.concatenate([a2[k].astype(F32) for k in range(NZ)], axis=1)

    part = mix_part(rows, gains[0:1, :], gate0[...], up0[...], down0[...])
    for k in range(NZ):
        b1s[k] = part[:, k * LANES : (k + 1) * LANES]
    parts_to_z(B1, b1s, b1r)
    b1r[z] = b1s[z]
    arrive(B1, b1r, NZ - 1)
    b2[yc] = total(b1r, NZ)
    to_yc(B2, b2)
    arrive(B2, b2, NYC - 1)
    stream_one = (res_z + total(b2, NYC)).astype(BF16).astype(F32)

    lane = iota((8, LANES), 1)
    mine = (lane >= y * 32) & (lane < y * 32 + 32)
    own = jnp.where(mine, stream_one, 0.0)
    squares = jnp.broadcast_to(jnp.sum(own * own, axis=1, keepdims=True), (8, LANES))
    gain_z = gains[1:2, pl.ds(pl.multiple_of(z * LANES, LANES), LANES)]
    scaled = (stream_one * gain_z).astype(BF16)
    qkv = jnp.dot(scaled, wpl[...], preferred_element_type=F32)
    for t in range(6):
        c1s[pl.ds(t, 8, stride=8), :] = qkv[:, t * LANES : (t + 1) * LANES]
    c1s[pl.ds(6, 8, stride=8), :] = squares
    c1s[pl.ds(7, 8, stride=8), :] = jnp.zeros((8, LANES), F32)
    for k in Y_STEPS:
        p = y_peer(k)
        send(C1, c1s.at[pl.ds(pl.multiple_of(p * 16, 16), 16)], c1r.at[y], {"kv_1": p})
    c1r[y] = c1s[pl.ds(pl.multiple_of(y * 16, 16), 16), :]
    arrive(C1, c1r, NY - 1)
    c2[z] = total(c1r, NY)
    to_z(C2, c2)
    arrive(C2, c2, NZ - 1)
    sums = total(c2, NZ)
    query_rows, key_rows, value_rows = [], [], []
    for s in range(2):
        block = sums[s * 8 : (s + 1) * 8]
        factor = lax.rsqrt(block[6:7] / D + EPS)
        block = (block * factor).astype(BF16).astype(F32)
        for g in range(4):
            query_rows += [block[g : g + 1], block[g : g + 1]]
        key_rows.append(jnp.broadcast_to(block[4:5], (8, LANES)))
        value_rows.append(jnp.broadcast_to(block[5:6], (8, LANES)))
    row16 = iota((16, LANES), 0)
    lane16 = iota((16, LANES), 1)
    component = lax.rem(row16, 2)
    queries = jnp.where((lane16 >= HEAD) == (component == 1), jnp.concatenate(query_rows, axis=0), 0.0)
    key_new = jnp.concatenate(key_rows, axis=0)
    value_new = jnp.concatenate(value_rows, axis=0)
    c3[y] = queries.astype(BF16)
    to_y(C3, c3)
    score_scale = HEAD**-0.5
    own_score = jnp.sum(queries * key_new, axis=1, keepdims=True) * score_scale
    loads[4].wait()
    loads[5].wait()
    arrive(C3, c3, NY - 1)

    span = kbuf.shape[1]
    position = (z * NY + y) * span + iota((8, span), 1)
    for b in range(8):
        query = c3[b // 2].astype(F32)[(b % 2) * 8 : (b % 2) * 8 + 8].astype(BF16)
        scores = lax.dot_general(query, kbuf[b], NT, preferred_element_type=F32) * score_scale
        alive = position < live[b]
        highest = jnp.max(jnp.where(alive, scores, -1e30), axis=1, keepdims=True)
        terms = jnp.where(alive, jnp.exp(scores - highest), 0.0)
        count = jnp.sum(terms, axis=1, keepdims=True)
        d1s[b // 2, (b % 2) * 8 : (b % 2) * 8 + 8, :] = jnp.dot(
            terms.astype(BF16), vbuf[b], preferred_element_type=F32
        )
        d1s[b // 2, 16 + (b % 2) * 8 : 24 + (b % 2) * 8, :] = jnp.where(lane < HEAD, highest, count)
    for k in Y_STEPS:
        p = y_peer(k)
        send(D1, d1s.at[p], d1r.at[y], {"kv_1": p})
    d1r[y] = d1s[y]
    arrive(D1, d1r, NY - 1)

    tops = [d1r[k, 16:32, 0:1] for k in range(NY)]
    counts = [d1r[k, 16:32, HEAD : HEAD + 1] for k in range(NY)]
    top = functools.reduce(jnp.maximum, tops)
    weights = [jnp.exp(t - top) for t in tops]
    count = sum(w * s for w, s in zip(weights, counts))
    values = sum(weights[k] * d1r[k, 0:16, :] for k in range(NY))
    d2o[z] = values.astype(BF16)
    line = jnp.where(lane16 == row16, top, 0.0) + jnp.where(lane16 == row16 + HEAD, count, 0.0)
    d2m[z] = jnp.sum(line, axis=0, keepdims=True)
    to_z(D2M, d2m)
    to_z(D2O, d2o)
    arrive(D2M, d2m, NZ - 1)
    tops = [
        jnp.sum(jnp.where(lane16 == row16, d2m[k], 0.0), axis=1, keepdims=True) for k in range(NZ)
    ]
    counts = [
        jnp.sum(jnp.where(lane16 == row16 + HEAD, d2m[k], 0.0), axis=1, keepdims=True) for k in range(NZ)
    ]
    top = functools.reduce(jnp.maximum, tops, own_score)
    weights = [jnp.exp(t - top) for t in tops]
    own_weight = jnp.exp(own_score - top)
    count = functools.reduce(jnp.add, [w * s for w, s in zip(weights, counts)], own_weight)
    arrive(D2O, d2o, NZ - 1)
    values = own_weight * value_new
    for k in range(NZ):
        values = values + weights[k] * d2o[k].astype(F32)
    ratio = values / count
    head = lax.rem(row16 // 2, 4)
    lambdas = jnp.where(
        head == 0, lam[0], jnp.where(head == 1, lam[1], jnp.where(head == 2, lam[2], lam[3]))
    )
    mixed = ratio - lambdas * pltpu.roll(ratio, 15, 0)
    scale = lax.rsqrt(jnp.mean(mixed * mixed, axis=1, keepdims=True) + EPS)
    heads = jnp.where(component == 0, mixed * scale * hgain[...], 0.0)
    d3[y] = heads.astype(BF16)
    to_y(D3, d3)
    arrive(D3, d3, NY - 1)

    heads = jnp.concatenate([d3[k].astype(F32) for k in range(NY)], axis=0)
    head = lax.rem(iota((64, LANES), 0) // 2, 4)
    wide = jnp.concatenate([jnp.where(head == g, heads, 0.0) for g in range(4)], axis=1).astype(BF16)
    projected = lax.dot_general(wide, popl[...], NT, preferred_element_type=F32)
    f1[yc] = jnp.sum(projected.reshape(8, 8, LANES), axis=1)
    to_yc(F1, f1)
    arrive(F1, f1, NYC - 1)
    stream_two = (stream_one + total(f1, NYC)).astype(BF16)
    f2[z] = stream_two
    to_z(F2, f2)
    arrive(F2, f2, NZ - 1)
    rows = jnp.concatenate([f2[k].astype(F32) for k in range(NZ)], axis=1)

    part = mix_part(rows, gains[2:3, :], gate1[...], up1[...], down1[...])
    for k in range(NZ):
        g1s[k] = part[:, k * LANES : (k + 1) * LANES].astype(g1s.dtype)
    parts_to_z(G1, g1s, g1r)
    g1r[z] = g1s[z]
    arrive(G1, g1r, NZ - 1)
    g2[yc] = total(g1r, NZ)
    to_yc(G2, g2)
    arrive(G2, g2, NYC - 1)
    updated = stream_two.astype(F32) + total(g2, NYC)
    out[...] = pltpu.roll(updated, lax.rem(LANES - own_lane, LANES), 1)[:, :16].astype(BF16)

    for whole in sent:
        whole.wait_send()


def local(
    residual, norm_gains, ffn_gate, ffn_up, ffn_down, proj_query, proj_key, proj_value, proj_out,
    head_lambda, head_gain, cache_keys, cache_values, live_length,
):
    batch = residual.shape[0]
    span = cache_keys.shape[1]
    vmem = pl.BlockSpec(memory_space=pltpu.VMEM)
    smem = pl.BlockSpec(memory_space=pltpu.SMEM)
    hbm = pl.BlockSpec(memory_space=pl.ANY)
    return pl.pallas_call(
        layer_kernel,
        out_shape=jax.ShapeDtypeStruct(residual.shape, BF16),
        in_specs=[vmem] * 8 + [hbm] * 4 + [smem, vmem, hbm, hbm, smem],
        out_specs=vmem,
        scratch_shapes=[
            pltpu.VMEM((32, 768), BF16),
            pltpu.VMEM((32, 512), BF16),
            pltpu.VMEM((batch, span, 128), BF16),
            pltpu.VMEM((batch, span, VDIM), BF16),
            pltpu.VMEM((LANES, 768), BF16),
            pltpu.VMEM((LANES, 512), BF16),
            pltpu.VMEM((NYC, 8, LANES), BF16),
            pltpu.VMEM((NZ, 8, LANES), BF16),
            pltpu.VMEM((NZ, 8, LANES), F32),
            pltpu.VMEM((NZ, 8, LANES), F32),
            pltpu.VMEM((NYC, 8, LANES), F32),
            pltpu.VMEM((64, LANES), F32),
            pltpu.VMEM((NY, 16, LANES), F32),
            pltpu.VMEM((NZ, 16, LANES), F32),
            pltpu.VMEM((NY, 16, LANES), BF16),
            pltpu.VMEM((NY, 32, LANES), F32),
            pltpu.VMEM((NY, 32, LANES), F32),
            pltpu.VMEM((NZ, 16, LANES), BF16),
            pltpu.VMEM((NZ, 1, LANES), F32),
            pltpu.VMEM((NY, 16, LANES), BF16),
            pltpu.VMEM((NYC, 8, LANES), F32),
            pltpu.VMEM((NZ, 8, LANES), BF16),
            pltpu.VMEM((NZ, 8, LANES), BF16),
            pltpu.VMEM((NZ, 8, LANES), BF16),
            pltpu.VMEM((NYC, 8, LANES), F32),
            pltpu.SemaphoreType.DMA((6,)),
            pltpu.SemaphoreType.DMA((15,)),
            pltpu.SemaphoreType.DMA((15,)),
        ],
        compiler_params=pltpu.CompilerParams(collective_id=0, has_side_effects=True),
    )(
        residual, norm_gains,
        ffn_gate[0], ffn_up[0], ffn_down[0], ffn_gate[1], ffn_up[1], ffn_down[1],
        proj_query, proj_key, proj_value, proj_out.T,
        head_lambda, head_gain.reshape(1, VDIM),
        cache_keys.reshape(batch, span, 128), cache_values.reshape(batch, span, VDIM), live_length,
    )


def solution(mesh):
    split = Mesh(
        mesh.devices.reshape(mesh.shape["dp"], NZ, NY, mesh.shape["tp"]),
        ("dp", "kv_0", "kv_1", "tp"),
    )
    return jax.shard_map(
        local,
        mesh=split,
        in_specs=(
            P("dp", KV_TP),
            P(),
            P(None, KV_TP, None),
            P(None, KV_TP, None),
            P(None, KV_TP, None),
            P(KV, "tp"),
            P(KV, "tp"),
            P(KV, "tp"),
            P("tp", KV),
            P("tp"),
            P(),
            P("dp", KV, "tp", None),
            P("dp", KV, "tp", None),
            P("dp"),
        ),
        out_specs=P("dp", KV_TP),
        check_vma=False,
    )
```

time: 273 us -> 101 us (0.37)
  blocking collectives: 159 us -> 0 us
  Pallas kernels: 0 us -> 93.7 us
  waiting for transfers between devices: 53.2 us -> 0 us
  starting transfers between devices: 35.9 us -> 0 us
  local copies, waits for them, and re-layouts: 15.3 us -> 6.89 us
  other arithmetic: 6.24 us -> 0 us
    pallas_call x0 -> x1, Pallas kernels: none -> 93.7 us  [local(): pl.pallas_call(layer_kernel, out_shape=jax.ShapeDtypeStruct(residual.shap...]
    all_to_all x7 -> x0, blocking collectives: 75.8 us -> none  [the longest x3 38.2 us: sent_and_summed(): lax.all_to_all(cut_along(value, dim, devices), axis, 0, 0, tiled=True)]
    all_to_all x4 -> x0, waiting for transfers between devices: 53.2 us -> none  [the longest x3 39.8 us: sent_to_all(): lax.all_to_all(jnp.broadcast_to(value[None], (devices, *value.shape)), ax...]
    psum x2 -> x0, blocking collectives: 51.3 us -> none  [by_axis(): value = lax.psum(value, axis)]
    all_to_all x4 -> x0, starting transfers between devices: 35.9 us -> none  [the longest x3 31.3 us: sent_to_all(): lax.all_to_all(jnp.broadcast_to(value[None], (devices, *value.shape)), ax...]
    all_gather x2 -> x0, blocking collectives: 31.5 us -> none  [all_in_one(): both, at, found = (lax.all_gather(jnp.concatenate(lines), axis), 0, {})]
    unnamed x39 -> x5, local copies, waits for them, and re-layouts: 4.38 us -> 1.28 us
  transfers between devices with their start and end apart: 4 -> 0, of which waited for: 4 -> 0; matrix products, arithmetic and copies ran while one was open for 1% -> 0% of each run, Pallas kernels for 0% -> 0%
where the time goes in v1:
time: 101 us
  Pallas kernels  93.7 us (93%)
  local copies, waits for them, and re-layouts  6.89 us (7%)
    pallas_call x1, Pallas kernels, local(): pl.pallas_call(layer_kernel, out_shape=jax.ShapeDtypeStruct(residual.shap...  93.7 us

profile of v1, /device:TPU:1, one launch (start us, length us, event | category | flops | bytes accessed | tf_op | source)
XLA Modules:
  0.0 100.6 jit_solution(16310083275107889046)
XLA Ops:
  0.0 1.7 %fusion.2 = (bf16[1,44,2048]{2,0,1:T(2,128)(2,1)S(1)}, bf16[1,44,2048]{2,0,1:T(2,128)(2,1)S(1)}) fusion(bf16[2,44,2048]{2,0,1:T(2,128)(2,1)} %param.16), kind=kLoop, calls=%fused_computation.8 | loop fusion | bytes 720896 | tf_op jit(solution)/shard_map/slice | solution.py:334
  1.7 0.0 copy-start
  1.7 1.0 copy_bitcast_fusion.2
  2.7 0.0 copy-done
  2.7 0.5 fusion.1
  3.2 0.0 copy-start.1
  3.2 1.0 copy_bitcast_fusion.1
  4.2 0.0 copy-done.1
  4.2 0.5 fusion
  4.7 1.0 copy_bitcast_fusion
  5.7 93.7 %shard_map.136 = bf16[8,16]{1,0:T(8,128)(2,1)} custom-call(bf16[8,16]{1,0:T(8,128)(2,1)} %res.1, f32[3,2048]{1,0:T(4,128)} %gains.1, bf16[44,2048]{1,0:T(8,128)(2,1)} %get-tuple-element.12.gate0, bf16[44,2048]{1,0:T(8,128)(2,1)} %get-tuple-element.14.up0, bf16[44,2048]{1,0:T(8,128)(2,1)} %get-tuple-element.16.down0, ...), custom_call_target="tpu_custom_call" | custom-call | tf_op jit(solution)/shard_map/pallas_call | solution.py:296
  99.4 1.2 %copy.34 = bf16[8,16]{1,0:T(8,128)(2,1)} copy(bf16[8,16]{1,0:T(8,128)(2,1)} %shard_map.136) | data formatting | bytes 512
Async XLA Ops:
  1.7 1.0 copy-start
  3.2 1.0 copy-start.1

commit v2 on v1

v2 whole, which is shorter than its diff:
```python
import functools

import jax
import jax.numpy as jnp
from jax import lax
from jax.experimental import pallas as pl
from jax.experimental.pallas import tpu as pltpu
from jax.sharding import Mesh
from jax.sharding import PartitionSpec as P

D = 2048
HEAD = 64
VDIM = 128
NZ = 16
NY = 4
NC = 2
NYC = NY * NC
LANES = 128
KV_TP = ("kv_0", "kv_1", "tp")
KV = ("kv_0", "kv_1")
MESH = pl.DeviceIdType.MESH
F32 = jnp.float32
BF16 = jnp.bfloat16
EPS = 1e-05
NT = (((1,), (1,)), ((), ()))

Z_STEPS = (8, 7, 9, 6, 10, 5, 11, 4, 12, 3, 13, 2, 14, 1, 15)
Y_STEPS = (2, 1, 3)
WEIGHT_ROWS = 48


def iota(shape, dim):
    return lax.broadcasted_iota(jnp.int32, shape, dim)


def mix_part(rows, gain, weights):
    scale = lax.rsqrt(jnp.mean(rows * rows, axis=1, keepdims=True) + EPS)
    normed = (rows * scale * gain).astype(BF16)
    gate = lax.dot_general(normed, weights[0], NT, preferred_element_type=F32)
    up = lax.dot_general(normed, weights[1], NT, preferred_element_type=F32)
    hidden = (gate / (1.0 + jnp.exp(-gate)) * up).astype(BF16)
    return 0.5 * jnp.dot(hidden, weights[2], preferred_element_type=F32)


def layer_kernel(
    res, gains, gate_h, up_h, down_h, wq_h, wk_h, wv_h, po_h, lam, hgain, ck_h, cv_h, live,
    out,
    raw, stage, wts, wqb, wkb, wvb, pob, lams, kbuf, vbuf,
    a1, a2, b1s, b1r, b2, cs, csq, c2, c3s, c3, d1s, d1r, d2o, d2m, hs, d3s, d3, ps, f2, fs, g1s, g1r, g2,
    hsem, ssem, rsem,
):
    z = lax.axis_index("kv_0")
    y = lax.axis_index("kv_1")
    c = lax.axis_index("tp")
    hidden_rows = raw.shape[1]
    barrier = pltpu.get_barrier_semaphore()
    drains = []

    def z_peer(k):
        return lax.rem(z + k, NZ)

    def y_peer(k):
        return lax.rem(y + k, NY)

    def send(s, r, src, dst, device):
        pltpu.make_async_remote_copy(
            src_ref=src, dst_ref=dst, send_sem=ssem.at[s], recv_sem=rsem.at[r],
            device_id=device, device_id_type=MESH,
        ).start()

    def waits(s, r, ref):
        return pltpu.make_async_remote_copy(
            src_ref=ref, dst_ref=ref, send_sem=ssem.at[s], recv_sem=rsem.at[r],
            device_id={"kv_0": z}, device_id_type=MESH,
        )

    def arrive(r, ref):
        waits(r, r, ref).wait_recv()

    def drain(s, ref):
        drains.append(waits(s, s, ref))

    def signal(device):
        pl.semaphore_signal(barrier, inc=1, device_id=device, device_id_type=MESH)

    def to_z(phase, src_of, dst):
        for k in Z_STEPS:
            p = z_peer(k)
            send(phase, phase, src_of(p), dst.at[z], {"kv_0": p})

    def to_y(phase, src, dst):
        for k in Y_STEPS:
            send(phase, phase, src, dst, {"kv_1": y_peer(k)})

    def total(buf, count):
        acc = buf[0].astype(F32)
        for k in range(1, count):
            acc = acc + buf[k].astype(F32)
        return acc

    def load(k):
        if k < 3:
            return pltpu.make_async_copy((gate_h, up_h, down_h)[k], raw.at[k], hsem.at[k])
        return pltpu.make_async_copy((ck_h, cv_h)[k - 3], (kbuf, vbuf)[k - 3], hsem.at[k])

    for k in range(5):
        load(k).start()

    def own_tile():
        spread = (iota((16, LANES), 1) == iota((16, LANES), 0) + (y * NC + c) * 16).astype(F32).astype(BF16)
        return jnp.dot(res[...], spread, preferred_element_type=F32).astype(BF16)

    lane = iota((8, LANES), 1)
    row = iota((8, LANES), 0)

    def own_lambdas():
        head = row // 2
        return jnp.where(head == 0, lam[0], jnp.where(head == 1, lam[1], jnp.where(head == 2, lam[2], lam[3])))

    def attend():
        span = kbuf.shape[1]
        position = (z * NY + y) * span + iota((8, span), 1)
        for b in range(8):
            query = c3[b // 2].astype(F32)[(b % 2) * 8 : (b % 2) * 8 + 8].astype(BF16)
            scores = lax.dot_general(query, kbuf[b], NT, preferred_element_type=F32) * HEAD**-0.5
            alive = position < live[b]
            highest = jnp.max(jnp.where(alive, scores, -1e30), axis=1, keepdims=True)
            terms = jnp.where(alive, jnp.exp(scores - highest), 0.0)
            count = jnp.sum(terms, axis=1, keepdims=True)
            d1s[b // 2, (b % 2) * 8 : (b % 2) * 8 + 8, :] = jnp.dot(
                terms.astype(BF16), vbuf[b], preferred_element_type=F32
            )
            d1s[b // 2, 16 + (b % 2) * 8 : 24 + (b % 2) * 8, :] = jnp.where(lane < HEAD, highest, count)

    def finish(stream_two):
        updated = stream_two.astype(F32) + total(g2, NY)
        out[...] = pltpu.roll(updated, lax.rem(LANES - (y * NC + c) * 16, LANES), 1)[:, :16]
        for each in drains:
            each.wait_send()
        drains.clear()

    @pl.when(c == 0)
    def _():
        core1 = {"tp": 1}

        def all_core1(s, r, src, dst):
            for k in Y_STEPS + (0,):
                send(s, r, src, dst, {"kv_1": y_peer(k), "tp": 1})

        for k in Y_STEPS + (0,):
            signal({"kv_1": y_peer(k), "tp": 1})
        a1[y * NC] = own_tile()
        lams[0] = own_lambdas()
        pl.semaphore_wait(barrier, NY)

        all_core1(A1, A1, a1.at[y * NC], a1.at[y * NC])
        drain(A1, a1.at[pl.ds(0, NY)])
        send(LAM, LAM, lams.at[0], lams.at[0], core1)
        drain(LAM, lams.at[0])
        stage[:, :, 40:WEIGHT_ROWS, :] = jnp.zeros((2, 3, WEIGHT_ROWS - 40, D), BF16)
        for half in range(2):
            for m in range(3):
                if half == 0:
                    load(m).wait()
                stage[half, m, 0:hidden_rows, :] = raw.at[m][:, half, :]
            for m in range(3):
                send(W0 + half, W0 + half, stage.at[half, m], wts.at[half, m, pl.ds(WEIGHT_ROWS, WEIGHT_ROWS)], core1)
            drain(W0 + half, stage.at[half])
            if half == 0:
                part = pl.ds(pl.multiple_of(y * 32, 32), 32)
                all_core1(WQ, WQ, wq_h, wqb.at[0, part])
                all_core1(WK, WK, wk_h, wkb.at[0, part])
                all_core1(WV, WV, wv_h, wvb.at[0, part])
                drain(WQ, wqb.at[0])
                drain(WK, wkb.at[0])
                drain(WV, wvb.at[0])
        all_core1(WO, WO, po_h, pob.at[part, pl.ds(0, 512)])
        drain(WO, pob.at[:, pl.ds(0, 512)])

        load(3).wait()
        load(4).wait()
        arrive(C3, c3)
        attend()
        for k in Y_STEPS + (0,):
            p = y_peer(k)
            send(D1, D1, d1s.at[p], d1r.at[y * NC], {"kv_1": p, "tp": 1})
        drain(D1, d1s)
        arrive(FS, fs)
        arrive(G2, g2)
        finish(fs[...])

    @pl.when(c == 1)
    def _():
        for k in Z_STEPS:
            signal({"kv_0": z_peer(k)})
        for k in Y_STEPS + (0,):
            signal({"kv_1": y_peer(k), "tp": 0})
        for k in Y_STEPS:
            signal({"kv_1": y_peer(k)})
        part = pl.ds(pl.multiple_of(y * 32, 32), 32)
        pulls = [
            pltpu.make_async_copy(wq_h, wqb.at[1, part], hsem.at[5]),
            pltpu.make_async_copy(wk_h, wkb.at[1, part], hsem.at[6]),
            pltpu.make_async_copy(wv_h, wvb.at[1, part], hsem.at[7]),
            pltpu.make_async_copy(po_h, pob.at[part, pl.ds(512, 512)], hsem.at[8]),
        ]
        for pull in pulls:
            pull.start()
        a1[y * NC + 1] = own_tile()
        lams[1] = own_lambdas()

        def relayout(half):
            for m in range(3):
                wts[half, m, 0:hidden_rows, :] = raw.at[m][:, half, :]

        wts[:, :, 40:WEIGHT_ROWS, :] = jnp.zeros((2, 3, WEIGHT_ROWS - 40, D), BF16)
        for m in range(3):
            load(m).wait()
        relayout(0)
        pl.semaphore_wait(barrier, (NZ - 1) + NY + (NY - 1))

        to_y(A1, a1.at[y * NC + 1], a1.at[y * NC + 1])
        drain(A1, a1.at[pl.ds(0, NY - 1)])
        arrive(A1, a1.at[pl.ds(0, NYC - 1)])
        res_z = total(a1, NYC)
        a2[z] = res_z.astype(BF16)
        to_z(A2, lambda p: a2.at[z], a2)
        drain(A2, a2.at[pl.ds(0, NZ - 1)])
        to_y(WQ, wq_h, wqb.at[1, part])
        to_y(WK, wk_h, wkb.at[1, part])
        to_y(WV, wv_h, wvb.at[1, part])
        to_y(WO, po_h, pob.at[part, pl.ds(512, 512)])
        drain(WQ, wqb.at[1, pl.ds(0, 96)])
        drain(WK, wkb.at[1, pl.ds(0, 96)])
        drain(WV, wvb.at[1, pl.ds(0, 96)])
        drain(WO, pob.at[pl.ds(0, 96), pl.ds(512, 512)])
        relayout(1)
        for pull in pulls:
            pull.wait()
        arrive(W0, wts.at[0, :, pl.ds(WEIGHT_ROWS, WEIGHT_ROWS)])
        arrive(A2, a2.at[pl.ds(0, NZ - 1)])
        rows = jnp.concatenate([a2[k].astype(F32) for k in range(NZ)], axis=1)

        mixed = mix_part(rows, gains[0:1, :], [wts[0, m] for m in range(3)])
        for k in range(NZ):
            b1s[k] = mixed[:, k * LANES : (k + 1) * LANES]
        to_z(B1, lambda p: b1s.at[p], b1r)
        drain(B1, b1s.at[pl.ds(0, NZ - 1)])
        b1r[z] = b1s[z]
        arrive(B1, b1r.at[pl.ds(0, NZ - 1)])
        b2[y] = total(b1r, NZ)
        to_y(B2, b2.at[y], b2.at[y])
        drain(B2, b2.at[pl.ds(0, NY - 1)])
        arrive(WQ, wqb.at[:, pl.ds(0, 112)])
        arrive(WK, wkb.at[:, pl.ds(0, 112)])
        arrive(WV, wvb.at[:, pl.ds(0, 112)])
        arrive(B2, b2.at[pl.ds(0, NY - 1)])
        stream_one = (res_z + total(b2, NY)).astype(BF16).astype(F32)

        squares = jnp.sum(stream_one * stream_one, axis=1, keepdims=True)
        csq[z] = jnp.sum(jnp.where(lane == row, squares, 0.0), axis=0, keepdims=True)
        to_z(CQ, lambda p: csq.at[z], csq)
        drain(CQ, csq.at[pl.ds(0, NZ - 1)])
        gain_z = gains[1:2, pl.ds(pl.multiple_of(z * LANES, LANES), LANES)]
        scaled = (stream_one * gain_z).astype(BF16)
        for t in range(2):
            query = jnp.dot(scaled, wqb[t], preferred_element_type=F32)
            for g in range(4):
                cs[pl.ds(t * 4 + g, 8, stride=12), :] = query[:, g * LANES : (g + 1) * LANES]
            cs[pl.ds(8 + t, 8, stride=12), :] = jnp.dot(scaled, wkb[t], preferred_element_type=F32)
            cs[pl.ds(10 + t, 8, stride=12), :] = jnp.dot(scaled, wvb[t], preferred_element_type=F32)
        pair = pl.ds(pl.multiple_of(y * 24, 8), 24)
        to_z(C2, lambda p: cs.at[pair], c2)
        drain(C2, c2.at[pl.ds(0, NZ - 1)])
        c2[z] = cs[pair, :]
        arrive(CQ, csq.at[pl.ds(0, NZ - 1)])
        square_line = total(csq, NZ)
        arrive(C2, c2.at[pl.ds(0, NZ - 1)])
        sums = total(c2, NZ)
        query_rows, key_rows, value_rows = [], [], []
        lane1 = iota((1, LANES), 1)
        for s in range(2):
            square = jnp.sum(jnp.where(lane1 == 2 * y + s, square_line, 0.0), axis=1, keepdims=True)
            factor = lax.rsqrt(square / D + EPS)
            block = (sums[s * 12 : (s + 1) * 12] * factor).astype(BF16).astype(F32)
            for h in range(8):
                query_rows += [block[h : h + 1], block[h : h + 1]]
            for t in range(2):
                key_rows.append(jnp.broadcast_to(block[8 + t : 9 + t], (8, LANES)))
                value_rows.append(jnp.broadcast_to(block[10 + t : 11 + t], (8, LANES)))
        row32 = iota((32, LANES), 0)
        lane32 = iota((32, LANES), 1)
        component = lax.rem(row32, 2)
        queries = jnp.where((lane32 >= HEAD) == (component == 1), jnp.concatenate(query_rows, axis=0), 0.0)
        for t in range(2):
            c3s[t] = jnp.concatenate(
                [queries[t * 8 : t * 8 + 8], queries[16 + t * 8 : 24 + t * 8]], axis=0
            ).astype(BF16)
        for k in Y_STEPS:
            send(C3S, C3, c3s.at[0], c3.at[y], {"kv_1": y_peer(k), "tp": 0})
            send(C3, C3, c3s.at[1], c3.at[y], {"kv_1": y_peer(k)})
        send(C3S, C3, c3s.at[0], c3.at[y], {"tp": 0})
        drain(C3S, c3)
        drain(C3, c3.at[pl.ds(0, NY - 1)])
        c3[y] = c3s[1]
        key_new = jnp.concatenate(key_rows, axis=0)
        value_new = jnp.concatenate(value_rows, axis=0)
        own_score = jnp.sum(queries * key_new, axis=1, keepdims=True) * HEAD**-0.5
        load(3).wait()
        load(4).wait()
        arrive(C3, c3.at[pl.ds(0, NY - 1)])
        attend()
        for k in Y_STEPS:
            p = y_peer(k)
            send(D1, D1, d1s.at[p], d1r.at[y * NC + 1], {"kv_1": p})
        drain(D1, d1s.at[pl.ds(0, NY - 1)])
        d1r[y * NC + 1] = d1s[y]
        arrive(LAM, lams.at[0])
        arrive(WO, pob.at[pl.ds(0, 112)])
        arrive(W1, wts.at[1, :, pl.ds(WEIGHT_ROWS, WEIGHT_ROWS)])
        arrive(D1, d1r.at[pl.ds(0, NYC - 1)])

        def gathered(k, start, lanes):
            return jnp.concatenate(
                [d1r[k * NC + t, start + s * 8 : start + s * 8 + 8, lanes] for s in range(2) for t in range(2)], axis=0
            )

        tops = [gathered(k, 16, slice(0, 1)) for k in range(NY)]
        counts = [gathered(k, 16, slice(HEAD, HEAD + 1)) for k in range(NY)]
        top = functools.reduce(jnp.maximum, tops)
        weights = [jnp.exp(t - top) for t in tops]
        count = functools.reduce(jnp.add, [w * s for w, s in zip(weights, counts)])
        values = functools.reduce(jnp.add, [weights[k] * gathered(k, 0, slice(None)) for k in range(NY)])
        line = jnp.where(lane32 == row32, top, 0.0) + jnp.where(lane32 == row32 + HEAD, count, 0.0)
        d2m[z] = jnp.sum(line, axis=0, keepdims=True)
        to_z(D2M, lambda p: d2m.at[z], d2m)
        drain(D2M, d2m.at[pl.ds(0, NZ - 1)])
        d2o[z] = values.astype(BF16)
        to_z(D2O, lambda p: d2o.at[z], d2o)
        drain(D2O, d2o.at[pl.ds(0, NZ - 1)])
        arrive(D2M, d2m.at[pl.ds(0, NZ - 1)])
        tops = [jnp.sum(jnp.where(lane32 == row32, d2m[k], 0.0), axis=1, keepdims=True) for k in range(NZ)]
        counts = [jnp.sum(jnp.where(lane32 == row32 + HEAD, d2m[k], 0.0), axis=1, keepdims=True) for k in range(NZ)]
        top = functools.reduce(jnp.maximum, tops, own_score)
        weights = [jnp.exp(t - top) for t in tops]
        own_weight = jnp.exp(own_score - top)
        count = functools.reduce(jnp.add, [w * s for w, s in zip(weights, counts)], own_weight)
        arrive(D2O, d2o.at[pl.ds(0, NZ - 1)])
        values = own_weight * value_new
        for k in range(NZ):
            values = values + weights[k] * d2o[k].astype(F32)
        ratio = values / count
        lambdas = jnp.concatenate([lams[0], lams[1], lams[0], lams[1]], axis=0)
        mixed = ratio - lambdas * pltpu.roll(ratio, 31, 0)
        scale = lax.rsqrt(jnp.mean(mixed * mixed, axis=1, keepdims=True) + EPS)
        hs[...] = mixed * scale * hgain[...]
        d3s[...] = hs[pl.ds(0, 16, stride=2), :].astype(BF16)
        to_y(D3, d3s, d3.at[y])
        drain(D3, d3.at[pl.ds(0, NY - 1)])
        d3[y] = d3s[...]
        arrive(D3, d3.at[pl.ds(0, NY - 1)])

        for k in range(NY):
            ps[k * 16 : (k + 1) * 16, :] = d3[k].astype(F32)
        heads = jnp.concatenate([ps[pl.ds(h, 8, stride=8), :] for h in range(8)], axis=1).astype(BF16)
        projected = lax.dot_general(heads, pob[...], NT, preferred_element_type=F32)
        stream_two = (stream_one + projected).astype(BF16)
        f2[z] = stream_two
        fs[...] = stream_two
        to_z(F2, lambda p: f2.at[z], f2)
        drain(F2, f2.at[pl.ds(0, NZ - 1)])
        send(FS, FS, fs, fs, {"tp": 0})
        drain(FS, fs)
        arrive(F2, f2.at[pl.ds(0, NZ - 1)])
        rows = jnp.concatenate([f2[k].astype(F32) for k in range(NZ)], axis=1)

        mixed = mix_part(rows, gains[2:3, :], [wts[1, m] for m in range(3)])
        for k in range(NZ):
            g1s[k] = mixed[:, k * LANES : (k + 1) * LANES]
        to_z(G1, lambda p: g1s.at[p], g1r)
        drain(G1, g1s.at[pl.ds(0, NZ - 1)])
        g1r[z] = g1s[z]
        arrive(G1, g1r.at[pl.ds(0, NZ - 1)])
        g2[y] = total(g1r, NZ)
        for k in Y_STEPS:
            send(G2S, G2, g2.at[y], g2.at[y], {"kv_1": y_peer(k), "tp": 0})
            send(G2, G2, g2.at[y], g2.at[y], {"kv_1": y_peer(k)})
        send(G2S, G2, g2.at[y], g2.at[y], {"tp": 0})
        drain(G2S, g2)
        drain(G2, g2.at[pl.ds(0, NY - 1)])
        arrive(G2, g2.at[pl.ds(0, NY - 1)])
        finish(stream_two)


PHASES = 28
(
    A1, A2, B1, B2, CQ, C2, C3, C3S, D1, D2O, D2M, D3, F2, FS, G1, G2, G2S, LAM, W0, W1, WQ, WK, WV, WO,
) = range(24)


def local(
    residual, norm_gains, ffn_gate, ffn_up, ffn_down, proj_query, proj_key, proj_value, proj_out,
    head_lambda, head_gain, cache_keys, cache_values, live_length,
):
    batch = residual.shape[0]
    hidden = ffn_gate.shape[1]
    span = cache_keys.shape[1]
    vmem = pl.BlockSpec(memory_space=pltpu.VMEM)
    smem = pl.BlockSpec(memory_space=pltpu.SMEM)
    hbm = pl.BlockSpec(memory_space=pl.ANY)
    updated = pl.pallas_call(
        layer_kernel,
        out_shape=jax.ShapeDtypeStruct(residual.shape, F32),
        in_specs=[vmem] * 2 + [hbm] * 7 + [smem, vmem, hbm, hbm, smem],
        out_specs=vmem,
        scratch_shapes=[
            pltpu.VMEM((3, hidden, 2, D), BF16),
            pltpu.VMEM((2, 3, WEIGHT_ROWS, D), BF16),
            pltpu.VMEM((2, 3, 2 * WEIGHT_ROWS, D), BF16),
            pltpu.VMEM((2, LANES, 512), BF16),
            pltpu.VMEM((2, LANES, 128), BF16),
            pltpu.VMEM((2, LANES, 128), BF16),
            pltpu.VMEM((LANES, 1024), BF16),
            pltpu.VMEM((2, 8, LANES), F32),
            pltpu.VMEM((batch, span, 128), BF16),
            pltpu.VMEM((batch, span, VDIM), BF16),
            pltpu.VMEM((NYC, 8, LANES), BF16),
            pltpu.VMEM((NZ, 8, LANES), BF16),
            pltpu.VMEM((NZ, 8, LANES), F32),
            pltpu.VMEM((NZ, 8, LANES), F32),
            pltpu.VMEM((NY, 8, LANES), F32),
            pltpu.VMEM((96, LANES), F32),
            pltpu.VMEM((NZ, 1, LANES), F32),
            pltpu.VMEM((NZ, 24, LANES), F32),
            pltpu.VMEM((2, 16, LANES), BF16),
            pltpu.VMEM((NY, 16, LANES), BF16),
            pltpu.VMEM((NY, 32, LANES), F32),
            pltpu.VMEM((NYC, 32, LANES), F32),
            pltpu.VMEM((NZ, 32, LANES), BF16),
            pltpu.VMEM((NZ, 1, LANES), F32),
            pltpu.VMEM((32, LANES), F32),
            pltpu.VMEM((16, LANES), BF16),
            pltpu.VMEM((NY, 16, LANES), BF16),
            pltpu.VMEM((64, LANES), F32),
            pltpu.VMEM((NZ, 8, LANES), BF16),
            pltpu.VMEM((8, LANES), BF16),
            pltpu.VMEM((NZ, 8, LANES), F32),
            pltpu.VMEM((NZ, 8, LANES), F32),
            pltpu.VMEM((NY, 8, LANES), F32),
            pltpu.SemaphoreType.DMA((9,)),
            pltpu.SemaphoreType.DMA((PHASES,)),
            pltpu.SemaphoreType.DMA((PHASES,)),
        ],
        compiler_params=pltpu.CompilerParams(collective_id=0, has_side_effects=True),
    )(
        residual, norm_gains,
        jnp.swapaxes(ffn_gate, 0, 1), jnp.swapaxes(ffn_up, 0, 1), jnp.swapaxes(ffn_down, 0, 1),
        proj_query, proj_key, proj_value, proj_out.T,
        head_lambda, head_gain.reshape(1, VDIM),
        cache_keys.reshape(batch, span, 128), cache_values.reshape(batch, span, VDIM), live_length,
    )
    return updated.astype(BF16)


def solution(mesh):
    split = Mesh(
        mesh.devices.reshape(mesh.shape["dp"], NZ, NY, mesh.shape["tp"]),
        ("dp", "kv_0", "kv_1", "tp"),
    )
    return jax.shard_map(
        local,
        mesh=split,
        in_specs=(
            P("dp", KV_TP),
            P(),
            P(None, KV_TP, None),
            P(None, KV_TP, None),
            P(None, KV_TP, None),
            P(KV, "tp"),
            P(KV, "tp"),
            P(KV, "tp"),
            P("tp", KV),
            P("tp"),
            P(),
            P("dp", KV, "tp", None),
            P("dp", KV, "tp", None),
            P("dp"),
        ),
        out_specs=P("dp", KV_TP),
        check_vma=False,
    )
```

time: 101 us -> 78.5 us (0.78)
  Pallas kernels: 93.7 us -> 77 us
  local copies, waits for them, and re-layouts: 6.89 us -> 0 us
  other arithmetic: 0 us -> 1.26 us
    pallas_call x1, Pallas kernels: 93.7 us -> 77 us  [local(): pl.pallas_call(layer_kernel, out_shape=jax.ShapeDtypeStruct(residual.shap...]
    squeeze x3 -> x0, local copies, waits for them, and re-layouts: 2.89 us -> none  [the longest x1 0.97 us: local(): ffn_down[1]]
    slice x3 -> x0, local copies, waits for them, and re-layouts: 2.71 us -> none  [the longest x1 1.71 us: local(): ffn_gate[1]]
    unnamed x5 -> x0, local copies, waits for them, and re-layouts: 1.28 us -> none
    convert_element_type x0 -> x1, other arithmetic: none -> 1.26 us  [local(): return updated.astype(BF16)]
where the time goes in v2:
time: 78.5 us; the launch traced here: 78.3 us
  Pallas kernels  77 us (98%)
  other arithmetic  1.26 us (2%)
    pallas_call x1, Pallas kernels, local(): pl.pallas_call(layer_kernel, out_shape=jax.ShapeDtypeStruct(residual.shap...  77 us

profile of v2, /device:TPU:1, one launch (start us, length us, event | category | flops | bytes accessed | tf_op | source)
XLA Modules:
  0.0 78.3 jit_solution(17531104518323099187)
XLA Ops:
  0.0 77.0 %shard_map.136 = f32[8,16]{1,0:T(8,128)} custom-call(bf16[8,16]{1,0:T(8,128)(2,1)} %res.1, f32[3,2048]{1,0:T(4,128)} %gains.1, bf16[44,2,2048]{2,1,0:T(2,128)(2,1)} %bitcast.9, bf16[44,2,2048]{2,1,0:T(2,128)(2,1)} %bitcast.10, bf16[44,2,2048]{2,1,0:T(2,128)(2,1)} %bitcast.11, bf16[32,512]{1,0:T(8,128)(2,1)} %wq_h.1, bf16[32,128]{1,0:T(8,128)(2,1)} %wk_h.1, ...), custom_call_target="tpu_custom_call" | custom-call | tf_op jit(solution)/shard_map/pallas_call | solution.py:411
  77.0 1.3 %convert_element_type.3 = bf16[8,16]{1,0:T(8,128)(2,1)} convert(f32[8,16]{1,0:T(8,128)} %shard_map.136) | non-fusion elementwise | flops 128 | bytes 768 | tf_op jit(solution)/shard_map/convert_element_type | solution.py:462

commit v3 on v2

--- a/solution.py
+++ b/solution.py
@@ -26,6 +26,8 @@
 
 Z_STEPS = (8, 7, 9, 6, 10, 5, 11, 4, 12, 3, 13, 2, 14, 1, 15)
 Y_STEPS = (2, 1, 3)
+REACH = 4
+NEAR_STEPS = (4, 12, 3, 13, 2, 14, 1, 15)
 WEIGHT_ROWS = 48
 
 
@@ -43,8 +45,9 @@
 
 
 def layer_kernel(
-    res, gains, gate_h, up_h, down_h, wq_h, wk_h, wv_h, po_h, lam, hgain, ck_h, cv_h, live,
+    res_h, gains_h, gate_h, up_h, down_h, wq_h, wk_h, wv_h, po_h, lam_h, hgain_h, ck_h, cv_h, live_h,
     out,
+    res, gains, lam, hgain, live,
     raw, stage, wts, wqb, wkb, wvb, pob, lams, kbuf, vbuf,
     a1, a2, b1s, b1r, b2, cs, csq, c2, c3s, c3, d1s, d1r, d2o, d2m, hs, d3s, d3, ps, f2, fs, g1s, g1r, g2,
     hsem, ssem, rsem,
@@ -101,9 +104,10 @@
     def load(k):
         if k < 3:
             return pltpu.make_async_copy((gate_h, up_h, down_h)[k], raw.at[k], hsem.at[k])
-        return pltpu.make_async_copy((ck_h, cv_h)[k - 3], (kbuf, vbuf)[k - 3], hsem.at[k])
-
-    for k in range(5):
+        src = (ck_h, cv_h, res_h, gains_h, lam_h, hgain_h, live_h)[k - 3]
+        return pltpu.make_async_copy(src, (kbuf, vbuf, res, gains, lam, hgain, live)[k - 3], hsem.at[k])
+
+    for k in (5, 7, 0, 1, 2, 6, 8, 9, 3, 4):
         load(k).start()
 
     def own_tile():
@@ -130,7 +134,10 @@
             d1s[b // 2, (b % 2) * 8 : (b % 2) * 8 + 8, :] = jnp.dot(
                 terms.astype(BF16), vbuf[b], preferred_element_type=F32
             )
-            d1s[b // 2, 16 + (b % 2) * 8 : 24 + (b % 2) * 8, :] = jnp.where(lane < HEAD, highest, count)
+            pair = jnp.where(lax.rem(lane, HEAD) < HEAD // 2, highest, count)
+            stats = pair if b % 2 == 0 else jnp.where(lane < HEAD, stats, pair)
+            if b % 2 == 1:
+                d1s[b // 2, 16:24, :] = stats
 
     def finish(stream_two):
         updated = stream_two.astype(F32) + total(g2, NY)
@@ -149,12 +156,14 @@
 
         for k in Y_STEPS + (0,):
             signal({"kv_1": y_peer(k), "tp": 1})
+        load(5).wait()
         a1[y * NC] = own_tile()
-        lams[0] = own_lambdas()
         pl.semaphore_wait(barrier, NY)
 
         all_core1(A1, A1, a1.at[y * NC], a1.at[y * NC])
         drain(A1, a1.at[pl.ds(0, NY)])
+        load(7).wait()
+        lams[0] = own_lambdas()
         send(LAM, LAM, lams.at[0], lams.at[0], core1)
         drain(LAM, lams.at[0])
         stage[:, :, 40:WEIGHT_ROWS, :] = jnp.zeros((2, 3, WEIGHT_ROWS - 40, D), BF16)
@@ -177,8 +186,8 @@
         all_core1(WO, WO, po_h, pob.at[part, pl.ds(0, 512)])
         drain(WO, pob.at[:, pl.ds(0, 512)])
 
-        load(3).wait()
-        load(4).wait()
+        for k in (3, 4, 6, 8, 9):
+            load(k).wait()
         arrive(C3, c3)
         attend()
         for k in Y_STEPS + (0,):
@@ -191,7 +200,7 @@
 
     @pl.when(c == 1)
     def _():
-        for k in Z_STEPS:
+        for k in NEAR_STEPS:
             signal({"kv_0": z_peer(k)})
         for k in Y_STEPS + (0,):
             signal({"kv_1": y_peer(k), "tp": 0})
@@ -199,15 +208,15 @@
             signal({"kv_1": y_peer(k)})
         part = pl.ds(pl.multiple_of(y * 32, 32), 32)
         pulls = [
-            pltpu.make_async_copy(wq_h, wqb.at[1, part], hsem.at[5]),
-            pltpu.make_async_copy(wk_h, wkb.at[1, part], hsem.at[6]),
-            pltpu.make_async_copy(wv_h, wvb.at[1, part], hsem.at[7]),
-            pltpu.make_async_copy(po_h, pob.at[part, pl.ds(512, 512)], hsem.at[8]),
+            pltpu.make_async_copy(wq_h, wqb.at[1, part], hsem.at[10]),
+            pltpu.make_async_copy(wk_h, wkb.at[1, part], hsem.at[11]),
+            pltpu.make_async_copy(wv_h, wvb.at[1, part], hsem.at[12]),
+            pltpu.make_async_copy(po_h, pob.at[part, pl.ds(512, 512)], hsem.at[13]),
         ]
         for pull in pulls:
             pull.start()
+        load(5).wait()
         a1[y * NC + 1] = own_tile()
-        lams[1] = own_lambdas()
 
         def relayout(half):
             for m in range(3):
@@ -217,15 +226,16 @@
         for m in range(3):
             load(m).wait()
         relayout(0)
-        pl.semaphore_wait(barrier, (NZ - 1) + NY + (NY - 1))
+        pl.semaphore_wait(barrier, len(NEAR_STEPS) + NY + (NY - 1))
 
         to_y(A1, a1.at[y * NC + 1], a1.at[y * NC + 1])
         drain(A1, a1.at[pl.ds(0, NY - 1)])
         arrive(A1, a1.at[pl.ds(0, NYC - 1)])
         res_z = total(a1, NYC)
         a2[z] = res_z.astype(BF16)
-        to_z(A2, lambda p: a2.at[z], a2)
-        drain(A2, a2.at[pl.ds(0, NZ - 1)])
+        for k in NEAR_STEPS:
+            send(A2, A2, a2.at[z], a2.at[z], {"kv_0": z_peer(k)})
+        drain(A2, a2.at[pl.ds(0, len(NEAR_STEPS))])
         to_y(WQ, wq_h, wqb.at[1, part])
         to_y(WK, wk_h, wkb.at[1, part])
         to_y(WV, wv_h, wvb.at[1, part])
@@ -234,11 +244,23 @@
         drain(WK, wkb.at[1, pl.ds(0, 96)])
         drain(WV, wvb.at[1, pl.ds(0, 96)])
         drain(WO, pob.at[pl.ds(0, 96), pl.ds(512, 512)])
+        load(7).wait()
+        lams[1] = own_lambdas()
+        arrive(A2, a2.at[pl.ds(0, len(NEAR_STEPS))])
+        for k in range(1, REACH + 1):
+            far = z_peer(NZ - k)
+            send(A3, A3, a2.at[far], a2.at[far], {"kv_0": z_peer(REACH)})
+            if k < REACH:
+                far = z_peer(k)
+                send(A3, A3, a2.at[far], a2.at[far], {"kv_0": z_peer(NZ - REACH)})
+        drain(A3, a2.at[pl.ds(0, 2 * REACH - 1)])
         relayout(1)
+        for k in (6, 8, 9):
+            load(k).wait()
         for pull in pulls:
             pull.wait()
         arrive(W0, wts.at[0, :, pl.ds(WEIGHT_ROWS, WEIGHT_ROWS)])
-        arrive(A2, a2.at[pl.ds(0, NZ - 1)])
+        arrive(A3, a2.at[pl.ds(0, 2 * REACH - 1)])
         rows = jnp.concatenate([a2[k].astype(F32) for k in range(NZ)], axis=1)
 
         mixed = mix_part(rows, gains[0:1, :], [wts[0, m] for m in range(3)])
@@ -320,17 +342,22 @@
         arrive(W1, wts.at[1, :, pl.ds(WEIGHT_ROWS, WEIGHT_ROWS)])
         arrive(D1, d1r.at[pl.ds(0, NYC - 1)])
 
-        def gathered(k, start, lanes):
+        both = [(s, t) for s in range(2) for t in range(2)]
+
+        def stat(k, at):
             return jnp.concatenate(
-                [d1r[k * NC + t, start + s * 8 : start + s * 8 + 8, lanes] for s in range(2) for t in range(2)], axis=0
+                [d1r[k * NC + t, 16:24, s * HEAD + at : s * HEAD + at + 1] for s, t in both], axis=0
             )
 
-        tops = [gathered(k, 16, slice(0, 1)) for k in range(NY)]
-        counts = [gathered(k, 16, slice(HEAD, HEAD + 1)) for k in range(NY)]
+        def gathered(k):
+            return jnp.concatenate([d1r[k * NC + t, s * 8 : s * 8 + 8, :] for s, t in both], axis=0)
+
+        tops = [stat(k, 0) for k in range(NY)]
+        counts = [stat(k, HEAD // 2) for k in range(NY)]
         top = functools.reduce(jnp.maximum, tops)
         weights = [jnp.exp(t - top) for t in tops]
         count = functools.reduce(jnp.add, [w * s for w, s in zip(weights, counts)])
-        values = functools.reduce(jnp.add, [weights[k] * gathered(k, 0, slice(None)) for k in range(NY)])
+        values = functools.reduce(jnp.add, [weights[k] * gathered(k) for k in range(NY)])
         line = jnp.where(lane32 == row32, top, 0.0) + jnp.where(lane32 == row32 + HEAD, count, 0.0)
         d2m[z] = jnp.sum(line, axis=0, keepdims=True)
         to_z(D2M, lambda p: d2m.at[z], d2m)
@@ -394,8 +421,8 @@
 
 PHASES = 28
 (
-    A1, A2, B1, B2, CQ, C2, C3, C3S, D1, D2O, D2M, D3, F2, FS, G1, G2, G2S, LAM, W0, W1, WQ, WK, WV, WO,
-) = range(24)
+    A1, A2, A3, B1, B2, CQ, C2, C3, C3S, D1, D2O, D2M, D3, F2, FS, G1, G2, G2S, LAM, W0, W1, WQ, WK, WV, WO,
+) = range(25)
 
 
 def local(
@@ -406,14 +433,18 @@
     hidden = ffn_gate.shape[1]
     span = cache_keys.shape[1]
     vmem = pl.BlockSpec(memory_space=pltpu.VMEM)
-    smem = pl.BlockSpec(memory_space=pltpu.SMEM)
     hbm = pl.BlockSpec(memory_space=pl.ANY)
     updated = pl.pallas_call(
         layer_kernel,
-        out_shape=jax.ShapeDtypeStruct(residual.shape, F32),
-        in_specs=[vmem] * 2 + [hbm] * 7 + [smem, vmem, hbm, hbm, smem],
+        out_shape=pltpu.VMEM(residual.shape, F32),
+        in_specs=[hbm] * 14,
         out_specs=vmem,
         scratch_shapes=[
+            pltpu.VMEM(residual.shape, BF16),
+            pltpu.VMEM(norm_gains.shape, F32),
+            pltpu.SMEM(head_lambda.shape, F32),
+            pltpu.VMEM((1, VDIM), F32),
+            pltpu.SMEM(live_length.shape, jnp.int32),
             pltpu.VMEM((3, hidden, 2, D), BF16),
             pltpu.VMEM((2, 3, WEIGHT_ROWS, D), BF16),
             pltpu.VMEM((2, 3, 2 * WEIGHT_ROWS, D), BF16),
@@ -434,8 +465,8 @@
             pltpu.VMEM((NZ, 24, LANES), F32),
             pltpu.VMEM((2, 16, LANES), BF16),
             pltpu.VMEM((NY, 16, LANES), BF16),
-            pltpu.VMEM((NY, 32, LANES), F32),
-            pltpu.VMEM((NYC, 32, LANES), F32),
+            pltpu.VMEM((NY, 24, LANES), F32),
+            pltpu.VMEM((NYC, 24, LANES), F32),
             pltpu.VMEM((NZ, 32, LANES), BF16),
             pltpu.VMEM((NZ, 1, LANES), F32),
             pltpu.VMEM((32, LANES), F32),
@@ -447,11 +478,13 @@
             pltpu.VMEM((NZ, 8, LANES), F32),
             pltpu.VMEM((NZ, 8, LANES), F32),
             pltpu.VMEM((NY, 8, LANES), F32),
-            pltpu.SemaphoreType.DMA((9,)),
+            pltpu.SemaphoreType.DMA((14,)),
             pltpu.SemaphoreType.DMA((PHASES,)),
             pltpu.SemaphoreType.DMA((PHASES,)),
         ],
-        compiler_params=pltpu.CompilerParams(collective_id=0, has_side_effects=True),
+        compiler_params=pltpu.CompilerParams(
+            collective_id=0, has_side_effects=True,
+        ),
     )(
         residual, norm_gains,
         jnp.swapaxes(ffn_gate, 0, 1), jnp.swapaxes(ffn_up, 0, 1), jnp.swapaxes(ffn_down, 0, 1),

time: 78.5 us -> 74.5 us (0.949)
  Pallas kernels: 77 us -> 73.8 us
    pallas_call x1, Pallas kernels: 77 us -> 73.8 us  [local(): pl.pallas_call(layer_kernel, out_shape=pltpu.VMEM(residual.shape, F32), i...]
where the time goes in v3:
time: 74.5 us; the launch traced here: 74.3 us
  Pallas kernels  73.8 us (99%)
    pallas_call x1, Pallas kernels, local(): pl.pallas_call(layer_kernel, out_shape=pltpu.VMEM(residual.shape, F32), i...  73.8 us

profile of v3, /device:TPU:1, one launch (start us, length us, event | category | flops | bytes accessed | tf_op | source)
XLA Modules:
  0.0 74.3 jit_solution(13774946081840749894)
XLA Ops:
  0.0 73.8 %shard_map.136 = f32[8,16]{1,0:T(8,128)S(1)} custom-call(bf16[8,16]{1,0:T(8,128)(2,1)} %res_h.1, f32[3,2048]{1,0:T(4,128)} %gains_h.1, bf16[44,2,2048]{2,1,0:T(2,128)(2,1)} %bitcast.9, bf16[44,2,2048]{2,1,0:T(2,128)(2,1)} %bitcast.10, bf16[44,2,2048]{2,1,0:T(2,128)(2,1)} %bitcast.11, bf16[32,512]{1,0:T(8,128)(2,1)} %wq_h.1, bf16[32,128]{1,0:T(8,128)(2,1)} %wk_h.1, ...), custom_call_target="tpu_custom_call" | custom-call | tf_op jit(solution)/shard_map/pallas_call | solution.py:437
  73.8 0.6 convert_element_type.3

commit v4 on v3

--- a/solution.py
+++ b/solution.py
@@ -28,6 +28,7 @@
 Y_STEPS = (2, 1, 3)
 REACH = 4
 NEAR_STEPS = (4, 12, 3, 13, 2, 14, 1, 15)
+FAR_STEPS = (8, 7, 9, 6, 10, 5, 11)
 WEIGHT_ROWS = 48
 
 
@@ -49,7 +50,7 @@
     out,
     res, gains, lam, hgain, live,
     raw, stage, wts, wqb, wkb, wvb, pob, lams, kbuf, vbuf,
-    a1, a2, b1s, b1r, b2, cs, csq, c2, c3s, c3, d1s, d1r, d2o, d2m, hs, d3s, d3, ps, f2, fs, g1s, g1r, g2,
+    a1, a2, b1s, b1r, b2, cs, ckvs, csq, c2, ckv, c3s, c3, d1s, d1r, d2o, d2m, hs, d3s, d3, ps, f2, fs, g1s, g1r, g2,
     hsem, ssem, rsem,
 ):
     z = lax.axis_index("kv_0")
@@ -62,6 +63,9 @@
     def z_peer(k):
         return lax.rem(z + k, NZ)
 
+    def lateness(p):
+        return jnp.minimum(p, NZ - p)
+
     def y_peer(k):
         return lax.rem(y + k, NY)
 
@@ -124,27 +128,42 @@
     def attend():
         span = kbuf.shape[1]
         position = (z * NY + y) * span + iota((8, span), 1)
-        for b in range(8):
-            query = c3[b // 2].astype(F32)[(b % 2) * 8 : (b % 2) * 8 + 8].astype(BF16)
-            scores = lax.dot_general(query, kbuf[b], NT, preferred_element_type=F32) * HEAD**-0.5
-            alive = position < live[b]
-            highest = jnp.max(jnp.where(alive, scores, -1e30), axis=1, keepdims=True)
-            terms = jnp.where(alive, jnp.exp(scores - highest), 0.0)
-            count = jnp.sum(terms, axis=1, keepdims=True)
-            d1s[b // 2, (b % 2) * 8 : (b % 2) * 8 + 8, :] = jnp.dot(
-                terms.astype(BF16), vbuf[b], preferred_element_type=F32
-            )
-            pair = jnp.where(lax.rem(lane, HEAD) < HEAD // 2, highest, count)
-            stats = pair if b % 2 == 0 else jnp.where(lane < HEAD, stats, pair)
-            if b % 2 == 1:
-                d1s[b // 2, 16:24, :] = stats
-
-    def finish(stream_two):
-        updated = stream_two.astype(F32) + total(g2, NY)
-        out[...] = pltpu.roll(updated, lax.rem(LANES - (y * NC + c) * 16, LANES), 1)[:, :16]
+        queries = jnp.concatenate([c3[k] for k in range(NY)], axis=0).astype(F32)
+        scores = jnp.concatenate(
+            [
+                lax.dot_general(
+                    queries[b * 8 : b * 8 + 8].astype(BF16), kbuf[b], NT, preferred_element_type=F32
+                )
+                for b in range(8)
+            ],
+            axis=0,
+        ) * HEAD**-0.5
+        alive = jnp.concatenate([(position < live[b]).astype(F32) for b in range(8)], axis=0) > 0.0
+        highest = jnp.max(jnp.where(alive, scores, -1e30), axis=1, keepdims=True)
+        terms = jnp.where(alive, jnp.exp(scores - highest), 0.0)
+        weights = terms.astype(BF16)
+        values = [jnp.dot(weights[b * 8 : b * 8 + 8], vbuf[b], preferred_element_type=F32) for b in range(8)]
+        count = jnp.sum(terms, axis=1, keepdims=True)
+        for k in range(NY):
+            pairs = [
+                jnp.where(
+                    lax.rem(lane, HEAD) < HEAD // 2, highest[b * 8 : b * 8 + 8], count[b * 8 : b * 8 + 8]
+                )
+                for b in (2 * k, 2 * k + 1)
+            ]
+            d1s[k, 0:8, :] = values[2 * k]
+            d1s[k, 8:16, :] = values[2 * k + 1]
+            d1s[k, 16:24, :] = jnp.where(lane < HEAD, pairs[0], pairs[1])
+
+    def sent_all():
         for each in drains:
             each.wait_send()
         drains.clear()
+
+    def finish(stream_two):
+        updated = stream_two.astype(F32) + total(g2, NY)
+        sent_all()
+        out[...] = pltpu.roll(updated, lax.rem(LANES - (y * NC + c) * 16, LANES), 1)[:, :16]
 
     @pl.when(c == 0)
     def _():
@@ -194,18 +213,28 @@
             p = y_peer(k)
             send(D1, D1, d1s.at[p], d1r.at[y * NC], {"kv_1": p, "tp": 1})
         drain(D1, d1s)
+        sent_all()
         arrive(FS, fs)
         arrive(G2, g2)
         finish(fs[...])
 
     @pl.when(c == 1)
     def _():
-        for k in NEAR_STEPS:
-            signal({"kv_0": z_peer(k)})
         for k in Y_STEPS + (0,):
             signal({"kv_1": y_peer(k), "tp": 0})
         for k in Y_STEPS:
             signal({"kv_1": y_peer(k)})
+        for k in NEAR_STEPS:
+            signal({"kv_0": z_peer(k)})
+        greeted = len(NEAR_STEPS) + NY + (NY - 1)
+        for k in FAR_STEPS:
+            p = z_peer(k)
+
+            @pl.when(lateness(z) <= lateness(p))
+            def _():
+                signal({"kv_0": p})
+
+            greeted = greeted + (lateness(p) <= lateness(z)).astype(jnp.int32)
         part = pl.ds(pl.multiple_of(y * 32, 32), 32)
         pulls = [
             pltpu.make_async_copy(wq_h, wqb.at[1, part], hsem.at[10]),
@@ -222,20 +251,32 @@
             for m in range(3):
                 wts[half, m, 0:hidden_rows, :] = raw.at[m][:, half, :]
 
+        pl.semaphore_wait(barrier, greeted)
+
+        to_y(A1, a1.at[y * NC + 1], a1.at[y * NC + 1])
+        drain(A1, a1.at[pl.ds(0, NY - 1)])
         wts[:, :, 40:WEIGHT_ROWS, :] = jnp.zeros((2, 3, WEIGHT_ROWS - 40, D), BF16)
         for m in range(3):
             load(m).wait()
         relayout(0)
-        pl.semaphore_wait(barrier, len(NEAR_STEPS) + NY + (NY - 1))
-
-        to_y(A1, a1.at[y * NC + 1], a1.at[y * NC + 1])
-        drain(A1, a1.at[pl.ds(0, NY - 1)])
         arrive(A1, a1.at[pl.ds(0, NYC - 1)])
         res_z = total(a1, NYC)
         a2[z] = res_z.astype(BF16)
-        for k in NEAR_STEPS:
-            send(A2, A2, a2.at[z], a2.at[z], {"kv_0": z_peer(k)})
-        drain(A2, a2.at[pl.ds(0, len(NEAR_STEPS))])
+        far_sends = 0
+        for k in FAR_STEPS:
+            p = z_peer(k)
+            known = lateness(z) >= lateness(p)
+
+            @pl.when(known)
+            def _():
+                send(A3, A3, a2.at[z], a2.at[z], {"kv_0": p})
+
+            far_sends = far_sends + known.astype(jnp.int32)
+        for k in range(REACH, 0, -1):
+            send(A2R, A2L, a2.at[z], a2.at[z], {"kv_0": z_peer(k)})
+            send(A2L, A2R, a2.at[z], a2.at[z], {"kv_0": z_peer(NZ - k)})
+        drain(A2R, a2.at[pl.ds(0, REACH)])
+        drain(A2L, a2.at[pl.ds(0, REACH)])
         to_y(WQ, wq_h, wqb.at[1, part])
         to_y(WK, wk_h, wkb.at[1, part])
         to_y(WV, wv_h, wvb.at[1, part])
@@ -246,14 +287,39 @@
         drain(WO, pob.at[pl.ds(0, 96), pl.ds(512, 512)])
         load(7).wait()
         lams[1] = own_lambdas()
-        arrive(A2, a2.at[pl.ds(0, len(NEAR_STEPS))])
+        def hand_on(side, beyond, target):
+            for k in range(1, beyond + 1):
+                block = z_peer(side * k + NZ)
+                asked = lateness(block) < lateness(target)
+
+                @pl.when(asked)
+                def _():
+                    send(A3, A3, a2.at[block], a2.at[block], {"kv_0": target})
+
+
+        def from_left():
+            arrive(A2L, a2.at[pl.ds(0, REACH)])
+            hand_on(-1, REACH, z_peer(REACH))
+
+        def from_right():
+            arrive(A2R, a2.at[pl.ds(0, REACH)])
+            hand_on(1, REACH - 1, z_peer(NZ - REACH))
+
+        @pl.when(z < NZ // 2)
+        def _():
+            from_left()
+            from_right()
+
+        @pl.when(z >= NZ // 2)
+        def _():
+            from_right()
+            from_left()
+
         for k in range(1, REACH + 1):
-            far = z_peer(NZ - k)
-            send(A3, A3, a2.at[far], a2.at[far], {"kv_0": z_peer(REACH)})
+            far_sends = far_sends + (lateness(z_peer(NZ - k)) < lateness(z_peer(REACH))).astype(jnp.int32)
             if k < REACH:
-                far = z_peer(k)
-                send(A3, A3, a2.at[far], a2.at[far], {"kv_0": z_peer(NZ - REACH)})
-        drain(A3, a2.at[pl.ds(0, 2 * REACH - 1)])
+                far_sends = far_sends + (lateness(z_peer(k)) < lateness(z_peer(NZ - REACH))).astype(jnp.int32)
+
         relayout(1)
         for k in (6, 8, 9):
             load(k).wait()
@@ -288,28 +354,30 @@
         for t in range(2):
             query = jnp.dot(scaled, wqb[t], preferred_element_type=F32)
             for g in range(4):
-                cs[pl.ds(t * 4 + g, 8, stride=12), :] = query[:, g * LANES : (g + 1) * LANES]
-            cs[pl.ds(8 + t, 8, stride=12), :] = jnp.dot(scaled, wkb[t], preferred_element_type=F32)
-            cs[pl.ds(10 + t, 8, stride=12), :] = jnp.dot(scaled, wvb[t], preferred_element_type=F32)
-        pair = pl.ds(pl.multiple_of(y * 24, 8), 24)
+                cs[pl.ds(t * 4 + g, 8, stride=8), :] = query[:, g * LANES : (g + 1) * LANES]
+        pair = pl.ds(pl.multiple_of(y * 16, 16), 16)
         to_z(C2, lambda p: cs.at[pair], c2)
         drain(C2, c2.at[pl.ds(0, NZ - 1)])
         c2[z] = cs[pair, :]
+        for t in range(2):
+            ckvs[pl.ds(t, 8, stride=4), :] = jnp.dot(scaled, wkb[t], preferred_element_type=F32)
+            ckvs[pl.ds(2 + t, 8, stride=4), :] = jnp.dot(scaled, wvb[t], preferred_element_type=F32)
+        pair_kv = pl.ds(pl.multiple_of(y * 8, 8), 8)
+        to_z(CKV, lambda p: ckvs.at[pair_kv], ckv)
+        drain(CKV, ckv.at[pl.ds(0, NZ - 1)])
+        ckv[z] = ckvs[pair_kv, :]
         arrive(CQ, csq.at[pl.ds(0, NZ - 1)])
         square_line = total(csq, NZ)
         arrive(C2, c2.at[pl.ds(0, NZ - 1)])
         sums = total(c2, NZ)
-        query_rows, key_rows, value_rows = [], [], []
+        query_rows, factors = [], []
         lane1 = iota((1, LANES), 1)
         for s in range(2):
             square = jnp.sum(jnp.where(lane1 == 2 * y + s, square_line, 0.0), axis=1, keepdims=True)
-            factor = lax.rsqrt(square / D + EPS)
-            block = (sums[s * 12 : (s + 1) * 12] * factor).astype(BF16).astype(F32)
+            factors.append(lax.rsqrt(square / D + EPS))
+            block = (sums[s * 8 : (s + 1) * 8] * factors[s]).astype(BF16).astype(F32)
             for h in range(8):
                 query_rows += [block[h : h + 1], block[h : h + 1]]
-            for t in range(2):
-                key_rows.append(jnp.broadcast_to(block[8 + t : 9 + t], (8, LANES)))
-                value_rows.append(jnp.broadcast_to(block[10 + t : 11 + t], (8, LANES)))
         row32 = iota((32, LANES), 0)
         lane32 = iota((32, LANES), 1)
         component = lax.rem(row32, 2)
@@ -325,9 +393,6 @@
         drain(C3S, c3)
         drain(C3, c3.at[pl.ds(0, NY - 1)])
         c3[y] = c3s[1]
-        key_new = jnp.concatenate(key_rows, axis=0)
-        value_new = jnp.concatenate(value_rows, axis=0)
-        own_score = jnp.sum(queries * key_new, axis=1, keepdims=True) * HEAD**-0.5
         load(3).wait()
         load(4).wait()
         arrive(C3, c3.at[pl.ds(0, NY - 1)])
@@ -337,6 +402,17 @@
             send(D1, D1, d1s.at[p], d1r.at[y * NC + 1], {"kv_1": p})
         drain(D1, d1s.at[pl.ds(0, NY - 1)])
         d1r[y * NC + 1] = d1s[y]
+        arrive(CKV, ckv.at[pl.ds(0, NZ - 1)])
+        sums = total(ckv, NZ)
+        key_rows, value_rows = [], []
+        for s in range(2):
+            block = (sums[s * 4 : s * 4 + 4] * factors[s]).astype(BF16).astype(F32)
+            for t in range(2):
+                key_rows.append(jnp.broadcast_to(block[t : t + 1], (8, LANES)))
+                value_rows.append(jnp.broadcast_to(block[2 + t : 3 + t], (8, LANES)))
+        key_new = jnp.concatenate(key_rows, axis=0)
+        value_new = jnp.concatenate(value_rows, axis=0)
+        own_score = jnp.sum(queries * key_new, axis=1, keepdims=True) * HEAD**-0.5
         arrive(LAM, lams.at[0])
         arrive(WO, pob.at[pl.ds(0, 112)])
         arrive(W1, wts.at[1, :, pl.ds(WEIGHT_ROWS, WEIGHT_ROWS)])
@@ -413,16 +489,22 @@
             send(G2S, G2, g2.at[y], g2.at[y], {"kv_1": y_peer(k), "tp": 0})
             send(G2, G2, g2.at[y], g2.at[y], {"kv_1": y_peer(k)})
         send(G2S, G2, g2.at[y], g2.at[y], {"tp": 0})
+        sent_all()
+
+        @pl.loop(0, far_sends)
+        def _(_):
+            waits(A3, A3, a2.at[0]).wait_send()
+
         drain(G2S, g2)
         drain(G2, g2.at[pl.ds(0, NY - 1)])
         arrive(G2, g2.at[pl.ds(0, NY - 1)])
         finish(stream_two)
 
 
-PHASES = 28
+PHASES = 27
 (
-    A1, A2, A3, B1, B2, CQ, C2, C3, C3S, D1, D2O, D2M, D3, F2, FS, G1, G2, G2S, LAM, W0, W1, WQ, WK, WV, WO,
-) = range(25)
+    A1, A2L, A2R, A3, B1, B2, CQ, C2, CKV, C3, C3S, D1, D2O, D2M, D3, F2, FS, G1, G2, G2S, LAM, W0, W1, WQ, WK, WV, WO,
+) = range(27)
 
 
 def local(
@@ -460,9 +542,11 @@
             pltpu.VMEM((NZ, 8, LANES), F32),
             pltpu.VMEM((NZ, 8, LANES), F32),
             pltpu.VMEM((NY, 8, LANES), F32),
-            pltpu.VMEM((96, LANES), F32),
+            pltpu.VMEM((64, LANES), F32),
+            pltpu.VMEM((32, LANES), F32),
             pltpu.VMEM((NZ, 1, LANES), F32),
-            pltpu.VMEM((NZ, 24, LANES), F32),
+            pltpu.VMEM((NZ, 16, LANES), F32),
+            pltpu.VMEM((NZ, 8, LANES), F32),
             pltpu.VMEM((2, 16, LANES), BF16),
             pltpu.VMEM((NY, 16, LANES), BF16),
             pltpu.VMEM((NY, 24, LANES), F32),

time: 74.5 us -> 74.6 us (level)
  no operation moved by 1% of the time
where the time goes in v4:
time: 74.6 us; the launch traced here: 74.5 us
  Pallas kernels  73.9 us (99%)
    pallas_call x1, Pallas kernels, local(): pl.pallas_call(layer_kernel, out_shape=pltpu.VMEM(residual.shape, F32), i...  73.9 us

profile of v4, /device:TPU:1, one launch (start us, length us, event | category | flops | bytes accessed | tf_op | source)
XLA Modules:
  0.0 74.5 jit_solution(7723523415605691654)
XLA Ops:
  0.0 73.9 %shard_map.136 = f32[8,16]{1,0:T(8,128)S(1)} custom-call(bf16[8,16]{1,0:T(8,128)(2,1)} %res_h.1, f32[3,2048]{1,0:T(4,128)} %gains_h.1, bf16[44,2,2048]{2,1,0:T(2,128)(2,1)} %bitcast.9, bf16[44,2,2048]{2,1,0:T(2,128)(2,1)} %bitcast.10, bf16[44,2,2048]{2,1,0:T(2,128)(2,1)} %bitcast.11, bf16[32,512]{1,0:T(8,128)(2,1)} %wq_h.1, bf16[32,128]{1,0:T(8,128)(2,1)} %wk_h.1, ...), custom_call_target="tpu_custom_call" | custom-call | tf_op jit(solution)/shard_map/pallas_call | solution.py:519
  73.9 0.6 convert_element_type.3

commit v5 on v4

--- a/solution.py
+++ b/solution.py
@@ -26,9 +26,6 @@
 
 Z_STEPS = (8, 7, 9, 6, 10, 5, 11, 4, 12, 3, 13, 2, 14, 1, 15)
 Y_STEPS = (2, 1, 3)
-REACH = 4
-NEAR_STEPS = (4, 12, 3, 13, 2, 14, 1, 15)
-FAR_STEPS = (8, 7, 9, 6, 10, 5, 11)
 WEIGHT_ROWS = 48
 
 
@@ -50,8 +47,8 @@
     out,
     res, gains, lam, hgain, live,
     raw, stage, wts, wqb, wkb, wvb, pob, lams, kbuf, vbuf,
-    a1, a2, b1s, b1r, b2, cs, ckvs, csq, c2, ckv, c3s, c3, d1s, d1r, d2o, d2m, hs, d3s, d3, ps, f2, fs, g1s, g1r, g2,
-    hsem, ssem, rsem,
+    a1, a2, b1s, b1r, b2, cs, ckvs, csq, c2, ckv, own, c3s, c3, d1s, d1r, d2o, d2m, hs, d3s, d3, ps, f2, fs, g1s, g1r, g2,
+    hsem, ssem, rsem, hello,
 ):
     z = lax.axis_index("kv_0")
     y = lax.axis_index("kv_1")
@@ -62,9 +59,6 @@
 
     def z_peer(k):
         return lax.rem(z + k, NZ)
-
-    def lateness(p):
-        return jnp.minimum(p, NZ - p)
 
     def y_peer(k):
         return lax.rem(y + k, NY)
@@ -173,11 +167,11 @@
             for k in Y_STEPS + (0,):
                 send(s, r, src, dst, {"kv_1": y_peer(k), "tp": 1})
 
-        for k in Y_STEPS + (0,):
-            signal({"kv_1": y_peer(k), "tp": 1})
         load(5).wait()
         a1[y * NC] = own_tile()
         pl.semaphore_wait(barrier, NY)
+        for k in Y_STEPS + (0,):
+            pl.semaphore_signal(hello, inc=1, device_id={"kv_1": y_peer(k), "tp": 1}, device_id_type=MESH)
 
         all_core1(A1, A1, a1.at[y * NC], a1.at[y * NC])
         drain(A1, a1.at[pl.ds(0, NY)])
@@ -222,19 +216,8 @@
     def _():
         for k in Y_STEPS + (0,):
             signal({"kv_1": y_peer(k), "tp": 0})
-        for k in Y_STEPS:
-            signal({"kv_1": y_peer(k)})
-        for k in NEAR_STEPS:
+        for k in Z_STEPS:
             signal({"kv_0": z_peer(k)})
-        greeted = len(NEAR_STEPS) + NY + (NY - 1)
-        for k in FAR_STEPS:
-            p = z_peer(k)
-
-            @pl.when(lateness(z) <= lateness(p))
-            def _():
-                signal({"kv_0": p})
-
-            greeted = greeted + (lateness(p) <= lateness(z)).astype(jnp.int32)
         part = pl.ds(pl.multiple_of(y * 32, 32), 32)
         pulls = [
             pltpu.make_async_copy(wq_h, wqb.at[1, part], hsem.at[10]),
@@ -251,7 +234,7 @@
             for m in range(3):
                 wts[half, m, 0:hidden_rows, :] = raw.at[m][:, half, :]
 
-        pl.semaphore_wait(barrier, greeted)
+        pl.semaphore_wait(hello, NY)
 
         to_y(A1, a1.at[y * NC + 1], a1.at[y * NC + 1])
         drain(A1, a1.at[pl.ds(0, NY - 1)])
@@ -262,21 +245,9 @@
         arrive(A1, a1.at[pl.ds(0, NYC - 1)])
         res_z = total(a1, NYC)
         a2[z] = res_z.astype(BF16)
-        far_sends = 0
-        for k in FAR_STEPS:
-            p = z_peer(k)
-            known = lateness(z) >= lateness(p)
-
-            @pl.when(known)
-            def _():
-                send(A3, A3, a2.at[z], a2.at[z], {"kv_0": p})
-
-            far_sends = far_sends + known.astype(jnp.int32)
-        for k in range(REACH, 0, -1):
-            send(A2R, A2L, a2.at[z], a2.at[z], {"kv_0": z_peer(k)})
-            send(A2L, A2R, a2.at[z], a2.at[z], {"kv_0": z_peer(NZ - k)})
-        drain(A2R, a2.at[pl.ds(0, REACH)])
-        drain(A2L, a2.at[pl.ds(0, REACH)])
+        pl.semaphore_wait(barrier, NZ - 1)
+        to_z(A2, lambda p: a2.at[z], a2)
+        drain(A2, a2.at[pl.ds(0, NZ - 1)])
         to_y(WQ, wq_h, wqb.at[1, part])
         to_y(WK, wk_h, wkb.at[1, part])
         to_y(WV, wv_h, wvb.at[1, part])
@@ -287,46 +258,13 @@
         drain(WO, pob.at[pl.ds(0, 96), pl.ds(512, 512)])
         load(7).wait()
         lams[1] = own_lambdas()
-        def hand_on(side, beyond, target):
-            for k in range(1, beyond + 1):
-                block = z_peer(side * k + NZ)
-                asked = lateness(block) < lateness(target)
-
-                @pl.when(asked)
-                def _():
-                    send(A3, A3, a2.at[block], a2.at[block], {"kv_0": target})
-
-
-        def from_left():
-            arrive(A2L, a2.at[pl.ds(0, REACH)])
-            hand_on(-1, REACH, z_peer(REACH))
-
-        def from_right():
-            arrive(A2R, a2.at[pl.ds(0, REACH)])
-            hand_on(1, REACH - 1, z_peer(NZ - REACH))
-
-        @pl.when(z < NZ // 2)
-        def _():
-            from_left()
-            from_right()
-
-        @pl.when(z >= NZ // 2)
-        def _():
-            from_right()
-            from_left()
-
-        for k in range(1, REACH + 1):
-            far_sends = far_sends + (lateness(z_peer(NZ - k)) < lateness(z_peer(REACH))).astype(jnp.int32)
-            if k < REACH:
-                far_sends = far_sends + (lateness(z_peer(k)) < lateness(z_peer(NZ - REACH))).astype(jnp.int32)
-
         relayout(1)
         for k in (6, 8, 9):
             load(k).wait()
         for pull in pulls:
             pull.wait()
         arrive(W0, wts.at[0, :, pl.ds(WEIGHT_ROWS, WEIGHT_ROWS)])
-        arrive(A3, a2.at[pl.ds(0, 2 * REACH - 1)])
+        arrive(A2, a2.at[pl.ds(0, NZ - 1)])
         rows = jnp.concatenate([a2[k].astype(F32) for k in range(NZ)], axis=1)
 
         mixed = mix_part(rows, gains[0:1, :], [wts[0, m] for m in range(3)])
@@ -363,9 +301,12 @@
             ckvs[pl.ds(t, 8, stride=4), :] = jnp.dot(scaled, wkb[t], preferred_element_type=F32)
             ckvs[pl.ds(2 + t, 8, stride=4), :] = jnp.dot(scaled, wvb[t], preferred_element_type=F32)
         pair_kv = pl.ds(pl.multiple_of(y * 8, 8), 8)
-        to_z(CKV, lambda p: ckvs.at[pair_kv], ckv)
-        drain(CKV, ckv.at[pl.ds(0, NZ - 1)])
-        ckv[z] = ckvs[pair_kv, :]
+        owner = y * NY
+
+        @pl.when(z != owner)
+        def _():
+            send(CKV, CKV, ckvs.at[pair_kv], ckv.at[z], {"kv_0": owner})
+
         arrive(CQ, csq.at[pl.ds(0, NZ - 1)])
         square_line = total(csq, NZ)
         arrive(C2, c2.at[pl.ds(0, NZ - 1)])
@@ -402,17 +343,27 @@
             send(D1, D1, d1s.at[p], d1r.at[y * NC + 1], {"kv_1": p})
         drain(D1, d1s.at[pl.ds(0, NY - 1)])
         d1r[y * NC + 1] = d1s[y]
-        arrive(CKV, ckv.at[pl.ds(0, NZ - 1)])
-        sums = total(ckv, NZ)
-        key_rows, value_rows = [], []
-        for s in range(2):
-            block = (sums[s * 4 : s * 4 + 4] * factors[s]).astype(BF16).astype(F32)
-            for t in range(2):
-                key_rows.append(jnp.broadcast_to(block[t : t + 1], (8, LANES)))
-                value_rows.append(jnp.broadcast_to(block[2 + t : 3 + t], (8, LANES)))
-        key_new = jnp.concatenate(key_rows, axis=0)
-        value_new = jnp.concatenate(value_rows, axis=0)
-        own_score = jnp.sum(queries * key_new, axis=1, keepdims=True) * HEAD**-0.5
+
+        @pl.when(z == owner)
+        def _():
+            ckv[z] = ckvs[pair_kv, :]
+            arrive(CKV, ckv.at[pl.ds(0, NZ - 1)])
+            sums = total(ckv, NZ)
+            key_rows, value_rows = [], []
+            for s in range(2):
+                block = (sums[s * 4 : s * 4 + 4] * factors[s]).astype(BF16).astype(F32)
+                for t in range(2):
+                    key_rows.append(jnp.broadcast_to(block[t : t + 1], (8, LANES)))
+                    value_rows.append(jnp.broadcast_to(block[2 + t : 3 + t], (8, LANES)))
+            products = queries * jnp.concatenate(key_rows, axis=0)
+            own[0] = jnp.broadcast_to(jnp.sum(products, axis=1, keepdims=True) * HEAD**-0.5, (32, LANES))
+            own[1] = jnp.concatenate(value_rows, axis=0)
+
+        @pl.when(z != owner)
+        def _():
+            own[0] = jnp.full((32, LANES), -1e30, F32)
+            own[1] = jnp.zeros((32, LANES), F32)
+
         arrive(LAM, lams.at[0])
         arrive(WO, pob.at[pl.ds(0, 112)])
         arrive(W1, wts.at[1, :, pl.ds(WEIGHT_ROWS, WEIGHT_ROWS)])
@@ -430,10 +381,13 @@
 
         tops = [stat(k, 0) for k in range(NY)]
         counts = [stat(k, HEAD // 2) for k in range(NY)]
-        top = functools.reduce(jnp.maximum, tops)
+        own_score = own[0, :, 0:1]
+        top = functools.reduce(jnp.maximum, tops, own_score)
         weights = [jnp.exp(t - top) for t in tops]
-        count = functools.reduce(jnp.add, [w * s for w, s in zip(weights, counts)])
-        values = functools.reduce(jnp.add, [weights[k] * gathered(k) for k in range(NY)])
+        own_weight = jnp.exp(own_score - top)
+        own_count = own_weight * (z == owner).astype(F32)
+        count = functools.reduce(jnp.add, [w * s for w, s in zip(weights, counts)], own_count)
+        values = functools.reduce(jnp.add, [weights[k] * gathered(k) for k in range(NY)], own_weight * own[1])
         line = jnp.where(lane32 == row32, top, 0.0) + jnp.where(lane32 == row32 + HEAD, count, 0.0)
         d2m[z] = jnp.sum(line, axis=0, keepdims=True)
         to_z(D2M, lambda p: d2m.at[z], d2m)
@@ -444,14 +398,11 @@
         arrive(D2M, d2m.at[pl.ds(0, NZ - 1)])
         tops = [jnp.sum(jnp.where(lane32 == row32, d2m[k], 0.0), axis=1, keepdims=True) for k in range(NZ)]
         counts = [jnp.sum(jnp.where(lane32 == row32 + HEAD, d2m[k], 0.0), axis=1, keepdims=True) for k in range(NZ)]
-        top = functools.reduce(jnp.maximum, tops, own_score)
+        top = functools.reduce(jnp.maximum, tops)
         weights = [jnp.exp(t - top) for t in tops]
-        own_weight = jnp.exp(own_score - top)
-        count = functools.reduce(jnp.add, [w * s for w, s in zip(weights, counts)], own_weight)
+        count = functools.reduce(jnp.add, [w * s for w, s in zip(weights, counts)])
         arrive(D2O, d2o.at[pl.ds(0, NZ - 1)])
-        values = own_weight * value_new
-        for k in range(NZ):
-            values = values + weights[k] * d2o[k].astype(F32)
+        values = functools.reduce(jnp.add, [weights[k] * d2o[k].astype(F32) for k in range(NZ)])
         ratio = values / count
         lambdas = jnp.concatenate([lams[0], lams[1], lams[0], lams[1]], axis=0)
         mixed = ratio - lambdas * pltpu.roll(ratio, 31, 0)
@@ -491,9 +442,9 @@
         send(G2S, G2, g2.at[y], g2.at[y], {"tp": 0})
         sent_all()
 
-        @pl.loop(0, far_sends)
-        def _(_):
-            waits(A3, A3, a2.at[0]).wait_send()
+        @pl.when(z != owner)
+        def _():
+            waits(CKV, CKV, ckv.at[0]).wait_send()
 
         drain(G2S, g2)
         drain(G2, g2.at[pl.ds(0, NY - 1)])
@@ -501,10 +452,10 @@
         finish(stream_two)
 
 
-PHASES = 27
+PHASES = 25
 (
-    A1, A2L, A2R, A3, B1, B2, CQ, C2, CKV, C3, C3S, D1, D2O, D2M, D3, F2, FS, G1, G2, G2S, LAM, W0, W1, WQ, WK, WV, WO,
-) = range(27)
+    A1, A2, B1, B2, CQ, C2, CKV, C3, C3S, D1, D2O, D2M, D3, F2, FS, G1, G2, G2S, LAM, W0, W1, WQ, WK, WV, WO,
+) = range(25)
 
 
 def local(
@@ -547,6 +498,7 @@
             pltpu.VMEM((NZ, 1, LANES), F32),
             pltpu.VMEM((NZ, 16, LANES), F32),
             pltpu.VMEM((NZ, 8, LANES), F32),
+            pltpu.VMEM((2, 32, LANES), F32),
             pltpu.VMEM((2, 16, LANES), BF16),
             pltpu.VMEM((NY, 16, LANES), BF16),
             pltpu.VMEM((NY, 24, LANES), F32),
@@ -565,6 +517,7 @@
             pltpu.SemaphoreType.DMA((14,)),
             pltpu.SemaphoreType.DMA((PHASES,)),
             pltpu.SemaphoreType.DMA((PHASES,)),
+            pltpu.SemaphoreType.REGULAR,
         ],
         compiler_params=pltpu.CompilerParams(
             collective_id=0, has_side_effects=True,

time: 74.6 us -> 70.9 us (0.950)
  Pallas kernels: 73.9 us -> 70.2 us
    pallas_call x1, Pallas kernels: 73.9 us -> 70.2 us  [local(): pl.pallas_call(layer_kernel, out_shape=pltpu.VMEM(residual.shape, F32), i...]
where the time goes in v5:
time: 70.9 us; the launch traced here: 70.8 us
  Pallas kernels  70.2 us (99%)
    pallas_call x1, Pallas kernels, local(): pl.pallas_call(layer_kernel, out_shape=pltpu.VMEM(residual.shape, F32), i...  70.2 us

profile of v5, /device:TPU:1, one launch (start us, length us, event | category | flops | bytes accessed | tf_op | source)
XLA Modules:
  0.0 70.8 jit_solution(1029097278369305890)
XLA Ops:
  0.0 70.2 %shard_map.136 = f32[8,16]{1,0:T(8,128)S(1)} custom-call(bf16[8,16]{1,0:T(8,128)(2,1)} %res_h.1, f32[3,2048]{1,0:T(4,128)} %gains_h.1, bf16[44,2,2048]{2,1,0:T(2,128)(2,1)} %bitcast.9, bf16[44,2,2048]{2,1,0:T(2,128)(2,1)} %bitcast.10, bf16[44,2,2048]{2,1,0:T(2,128)(2,1)} %bitcast.11, bf16[32,512]{1,0:T(8,128)(2,1)} %wq_h.1, bf16[32,128]{1,0:T(8,128)(2,1)} %wk_h.1, ...), custom_call_target="tpu_custom_call" | custom-call | tf_op jit(solution)/shard_map/pallas_call | solution.py:470
  70.2 0.6 convert_element_type.3

commit v6 on v5

--- a/solution.py
+++ b/solution.py
@@ -105,8 +105,9 @@
         src = (ck_h, cv_h, res_h, gains_h, lam_h, hgain_h, live_h)[k - 3]
         return pltpu.make_async_copy(src, (kbuf, vbuf, res, gains, lam, hgain, live)[k - 3], hsem.at[k])
 
-    for k in (5, 7, 0, 1, 2, 6, 8, 9, 3, 4):
-        load(k).start()
+    def start_loads():
+        for k in (5, 0, 1, 2, 7, 6, 8, 9, 3, 4):
+            load(k).start()
 
     def own_tile():
         spread = (iota((16, LANES), 1) == iota((16, LANES), 0) + (y * NC + c) * 16).astype(F32).astype(BF16)
@@ -167,11 +168,11 @@
             for k in Y_STEPS + (0,):
                 send(s, r, src, dst, {"kv_1": y_peer(k), "tp": 1})
 
+        start_loads()
         load(5).wait()
         a1[y * NC] = own_tile()
         pl.semaphore_wait(barrier, NY)
-        for k in Y_STEPS + (0,):
-            pl.semaphore_signal(hello, inc=1, device_id={"kv_1": y_peer(k), "tp": 1}, device_id_type=MESH)
+        pl.semaphore_signal(hello, inc=1, device_id=core1, device_id_type=MESH)
 
         all_core1(A1, A1, a1.at[y * NC], a1.at[y * NC])
         drain(A1, a1.at[pl.ds(0, NY)])
@@ -214,10 +215,11 @@
 
     @pl.when(c == 1)
     def _():
+        for k in Z_STEPS:
+            signal({"kv_0": z_peer(k)})
         for k in Y_STEPS + (0,):
             signal({"kv_1": y_peer(k), "tp": 0})
-        for k in Z_STEPS:
-            signal({"kv_0": z_peer(k)})
+        start_loads()
         part = pl.ds(pl.multiple_of(y * 32, 32), 32)
         pulls = [
             pltpu.make_async_copy(wq_h, wqb.at[1, part], hsem.at[10]),
@@ -234,7 +236,7 @@
             for m in range(3):
                 wts[half, m, 0:hidden_rows, :] = raw.at[m][:, half, :]
 
-        pl.semaphore_wait(hello, NY)
+        pl.semaphore_wait(hello, 1)
 
         to_y(A1, a1.at[y * NC + 1], a1.at[y * NC + 1])
         drain(A1, a1.at[pl.ds(0, NY - 1)])
@@ -283,18 +285,20 @@
         arrive(B2, b2.at[pl.ds(0, NY - 1)])
         stream_one = (res_z + total(b2, NY)).astype(BF16).astype(F32)
 
+        gain_z = gains[1:2, pl.ds(pl.multiple_of(z * LANES, LANES), LANES)]
+        scaled = (stream_one * gain_z).astype(BF16)
+        query = [jnp.dot(scaled, wqb[t], preferred_element_type=F32) for t in range(2)]
         squares = jnp.sum(stream_one * stream_one, axis=1, keepdims=True)
         csq[z] = jnp.sum(jnp.where(lane == row, squares, 0.0), axis=0, keepdims=True)
-        to_z(CQ, lambda p: csq.at[z], csq)
+        for t in range(2):
+            for g in range(4):
+                cs[pl.ds(t * 4 + g, 8, stride=8), :] = query[t][:, g * LANES : (g + 1) * LANES]
+        pair = pl.ds(pl.multiple_of(y * 16, 16), 16)
+        for k in Z_STEPS:
+            p = z_peer(k)
+            send(CQ, CQ, csq.at[z], csq.at[z], {"kv_0": p})
+            send(C2, C2, cs.at[pair], c2.at[z], {"kv_0": p})
         drain(CQ, csq.at[pl.ds(0, NZ - 1)])
-        gain_z = gains[1:2, pl.ds(pl.multiple_of(z * LANES, LANES), LANES)]
-        scaled = (stream_one * gain_z).astype(BF16)
-        for t in range(2):
-            query = jnp.dot(scaled, wqb[t], preferred_element_type=F32)
-            for g in range(4):
-                cs[pl.ds(t * 4 + g, 8, stride=8), :] = query[:, g * LANES : (g + 1) * LANES]
-        pair = pl.ds(pl.multiple_of(y * 16, 16), 16)
-        to_z(C2, lambda p: cs.at[pair], c2)
         drain(C2, c2.at[pl.ds(0, NZ - 1)])
         c2[z] = cs[pair, :]
         for t in range(2):
@@ -356,48 +360,58 @@
                     key_rows.append(jnp.broadcast_to(block[t : t + 1], (8, LANES)))
                     value_rows.append(jnp.broadcast_to(block[2 + t : 3 + t], (8, LANES)))
             products = queries * jnp.concatenate(key_rows, axis=0)
-            own[0] = jnp.broadcast_to(jnp.sum(products, axis=1, keepdims=True) * HEAD**-0.5, (32, LANES))
-            own[1] = jnp.concatenate(value_rows, axis=0)
+            scores = jnp.sum(products, axis=1, keepdims=True) * HEAD**-0.5
+            for t in range(2):
+                pair = jnp.where(lane < HEAD, scores[t * 8 : t * 8 + 8], scores[16 + t * 8 : 24 + t * 8])
+                own[t] = jnp.where(lax.rem(lane, HEAD) < HEAD // 2, pair, 1.0)
+            for k in range(4):
+                own[2 + k] = value_rows[k]
 
         @pl.when(z != owner)
         def _():
-            own[0] = jnp.full((32, LANES), -1e30, F32)
-            own[1] = jnp.zeros((32, LANES), F32)
+            for t in range(2):
+                own[t] = jnp.where(lax.rem(lane, HEAD) < HEAD // 2, -1e30, 0.0)
+            for k in range(4):
+                own[2 + k] = jnp.zeros((8, LANES), F32)
 
         arrive(LAM, lams.at[0])
         arrive(WO, pob.at[pl.ds(0, 112)])
         arrive(W1, wts.at[1, :, pl.ds(WEIGHT_ROWS, WEIGHT_ROWS)])
         arrive(D1, d1r.at[pl.ds(0, NYC - 1)])
 
-        both = [(s, t) for s in range(2) for t in range(2)]
-
-        def stat(k, at):
-            return jnp.concatenate(
-                [d1r[k * NC + t, 16:24, s * HEAD + at : s * HEAD + at + 1] for s, t in both], axis=0
+        is_top = lax.rem(lane, HEAD) < HEAD // 2
+        joined, line = [[], []], jnp.zeros((1, LANES), F32)
+        for t in range(2):
+            stats = [d1r[k * NC + t, 16:24, :] for k in range(NY)] + [own[t]]
+            blocks = [[d1r[k * NC + t, s * 8 : s * 8 + 8, :] for s in range(2)] for k in range(NY)]
+            blocks += [[own[2 + t], own[4 + t]]]
+            top = functools.reduce(jnp.maximum, stats)
+            weights = [jnp.where(is_top, jnp.exp(jnp.where(is_top, each - top, 0.0)), 0.0) for each in stats]
+            count = functools.reduce(
+                jnp.add, [pltpu.roll(w, HEAD // 2, 1) * each for w, each in zip(weights, stats)]
             )
-
-        def gathered(k):
-            return jnp.concatenate([d1r[k * NC + t, s * 8 : s * 8 + 8, :] for s, t in both], axis=0)
-
-        tops = [stat(k, 0) for k in range(NY)]
-        counts = [stat(k, HEAD // 2) for k in range(NY)]
-        own_score = own[0, :, 0:1]
-        top = functools.reduce(jnp.maximum, tops, own_score)
-        weights = [jnp.exp(t - top) for t in tops]
-        own_weight = jnp.exp(own_score - top)
-        own_count = own_weight * (z == owner).astype(F32)
-        count = functools.reduce(jnp.add, [w * s for w, s in zip(weights, counts)], own_count)
-        values = functools.reduce(jnp.add, [weights[k] * gathered(k) for k in range(NY)], own_weight * own[1])
-        line = jnp.where(lane32 == row32, top, 0.0) + jnp.where(lane32 == row32 + HEAD, count, 0.0)
-        d2m[z] = jnp.sum(line, axis=0, keepdims=True)
-        to_z(D2M, lambda p: d2m.at[z], d2m)
+            packed = jnp.where(is_top, top, count)
+            line += jnp.sum(jnp.where(lax.rem(lane, HEAD // 2) == row + t * 8, packed, 0.0), axis=0, keepdims=True)
+            for s in range(2):
+                joined[s].append(
+                    functools.reduce(
+                        jnp.add, [w[:, s * HEAD : s * HEAD + 1] * each[s] for w, each in zip(weights, blocks)]
+                    )
+                )
+        d2m[z] = line
+        d2o[z] = jnp.concatenate(joined[0] + joined[1], axis=0).astype(BF16)
+        for k in Z_STEPS:
+            p = z_peer(k)
+            send(D2M, D2M, d2m.at[z], d2m.at[z], {"kv_0": p})
+            send(D2O, D2O, d2o.at[z], d2o.at[z], {"kv_0": p})
         drain(D2M, d2m.at[pl.ds(0, NZ - 1)])
-        d2o[z] = values.astype(BF16)
-        to_z(D2O, lambda p: d2o.at[z], d2o)
         drain(D2O, d2o.at[pl.ds(0, NZ - 1)])
         arrive(D2M, d2m.at[pl.ds(0, NZ - 1)])
-        tops = [jnp.sum(jnp.where(lane32 == row32, d2m[k], 0.0), axis=1, keepdims=True) for k in range(NZ)]
-        counts = [jnp.sum(jnp.where(lane32 == row32 + HEAD, d2m[k], 0.0), axis=1, keepdims=True) for k in range(NZ)]
+        spot = row32 // 16 * HEAD + lax.rem(row32, 16)
+        tops = [jnp.sum(jnp.where(lane32 == spot, d2m[k], 0.0), axis=1, keepdims=True) for k in range(NZ)]
+        counts = [
+            jnp.sum(jnp.where(lane32 == spot + HEAD // 2, d2m[k], 0.0), axis=1, keepdims=True) for k in range(NZ)
+        ]
         top = functools.reduce(jnp.maximum, tops)
         weights = [jnp.exp(t - top) for t in tops]
         count = functools.reduce(jnp.add, [w * s for w, s in zip(weights, counts)])
@@ -498,7 +512,7 @@
             pltpu.VMEM((NZ, 1, LANES), F32),
             pltpu.VMEM((NZ, 16, LANES), F32),
             pltpu.VMEM((NZ, 8, LANES), F32),
-            pltpu.VMEM((2, 32, LANES), F32),
+            pltpu.VMEM((6, 8, LANES), F32),
             pltpu.VMEM((2, 16, LANES), BF16),
             pltpu.VMEM((NY, 16, LANES), BF16),
             pltpu.VMEM((NY, 24, LANES), F32),

time: 70.9 us -> 70.9 us (level)
  no operation moved by 1% of the time
where the time goes in v6:
time: 70.9 us; the launch traced here: 70.7 us
  Pallas kernels  70.1 us (99%)
    pallas_call x1, Pallas kernels, local(): pl.pallas_call(layer_kernel, out_shape=pltpu.VMEM(residual.shape, F32), i...  70.1 us

profile of v6, /device:TPU:1, one launch (start us, length us, event | category | flops | bytes accessed | tf_op | source)
XLA Modules:
  0.0 70.7 jit_solution(15522626911569496504)
XLA Ops:
  0.0 70.1 %shard_map.136 = f32[8,16]{1,0:T(8,128)S(1)} custom-call(bf16[8,16]{1,0:T(8,128)(2,1)} %res_h.1, f32[3,2048]{1,0:T(4,128)} %gains_h.1, bf16[44,2,2048]{2,1,0:T(2,128)(2,1)} %bitcast.9, bf16[44,2,2048]{2,1,0:T(2,128)(2,1)} %bitcast.10, bf16[44,2,2048]{2,1,0:T(2,128)(2,1)} %bitcast.11, bf16[32,512]{1,0:T(8,128)(2,1)} %wq_h.1, bf16[32,128]{1,0:T(8,128)(2,1)} %wk_h.1, ...), custom_call_target="tpu_custom_call" | custom-call | tf_op jit(solution)/shard_map/pallas_call | solution.py:484
  70.2 0.6 convert_element_type.3

commit v7 on v6

--- a/solution.py
+++ b/solution.py
@@ -103,7 +103,9 @@
         if k < 3:
             return pltpu.make_async_copy((gate_h, up_h, down_h)[k], raw.at[k], hsem.at[k])
         src = (ck_h, cv_h, res_h, gains_h, lam_h, hgain_h, live_h)[k - 3]
-        return pltpu.make_async_copy(src, (kbuf, vbuf, res, gains, lam, hgain, live)[k - 3], hsem.at[k])
+        if k < 5:
+            src = src.at[pl.ds(2 * y, 2)]
+        return pltpu.make_async_copy(src, (kbuf.at[y], vbuf.at[y], res, gains, lam, hgain, live)[k - 3], hsem.at[k])
 
     def start_loads():
         for k in (5, 0, 1, 2, 7, 6, 8, 9, 3, 4):
@@ -120,24 +122,26 @@
         head = row // 2
         return jnp.where(head == 0, lam[0], jnp.where(head == 1, lam[1], jnp.where(head == 2, lam[2], lam[3])))
 
-    def attend():
-        span = kbuf.shape[1]
-        position = (z * NY + y) * span + iota((8, span), 1)
-        queries = jnp.concatenate([c3[k] for k in range(NY)], axis=0).astype(F32)
+    def attend(tile):
+        span = kbuf.shape[2]
+        queries = tile.astype(F32)
+        queries = [queries[t * 8 : t * 8 + 8].astype(BF16) for t in range(2)]
         scores = jnp.concatenate(
             [
-                lax.dot_general(
-                    queries[b * 8 : b * 8 + 8].astype(BF16), kbuf[b], NT, preferred_element_type=F32
-                )
+                lax.dot_general(queries[b % 2], kbuf[b // 2, b % 2], NT, preferred_element_type=F32)
                 for b in range(8)
             ],
             axis=0,
         ) * HEAD**-0.5
-        alive = jnp.concatenate([(position < live[b]).astype(F32) for b in range(8)], axis=0) > 0.0
+        place = z * NY * span + iota((8, span), 1)
+        length = [live[2 * y], live[2 * y + 1]]
+        alive = jnp.concatenate(
+            [(place + (b // 2) * span < length[b % 2]).astype(F32) for b in range(8)], axis=0
+        ) > 0.0
         highest = jnp.max(jnp.where(alive, scores, -1e30), axis=1, keepdims=True)
         terms = jnp.where(alive, jnp.exp(scores - highest), 0.0)
         weights = terms.astype(BF16)
-        values = [jnp.dot(weights[b * 8 : b * 8 + 8], vbuf[b], preferred_element_type=F32) for b in range(8)]
+        values = [jnp.dot(weights[b * 8 : b * 8 + 8], vbuf[b // 2, b % 2], preferred_element_type=F32) for b in range(8)]
         count = jnp.sum(terms, axis=1, keepdims=True)
         for k in range(NY):
             pairs = [
@@ -150,6 +154,12 @@
             d1s[k, 8:16, :] = values[2 * k + 1]
             d1s[k, 16:24, :] = jnp.where(lane < HEAD, pairs[0], pairs[1])
 
+    def give(phase, cache, buf):
+        for k in Y_STEPS:
+            p = y_peer(k)
+            send(phase, phase, cache.at[pl.ds(2 * p, 2)], buf.at[y], {"kv_1": p})
+        drain(phase, buf.at[pl.ds(0, NY - 1)])
+
     def sent_all():
         for each in drains:
             each.wait_send()
@@ -168,10 +178,12 @@
             for k in Y_STEPS + (0,):
                 send(s, r, src, dst, {"kv_1": y_peer(k), "tp": 1})
 
+        for k in Y_STEPS:
+            signal({"kv_1": y_peer(k)})
         start_loads()
         load(5).wait()
         a1[y * NC] = own_tile()
-        pl.semaphore_wait(barrier, NY)
+        pl.semaphore_wait(barrier, NY + NY - 1)
         pl.semaphore_signal(hello, inc=1, device_id=core1, device_id_type=MESH)
 
         all_core1(A1, A1, a1.at[y * NC], a1.at[y * NC])
@@ -181,32 +193,36 @@
         send(LAM, LAM, lams.at[0], lams.at[0], core1)
         drain(LAM, lams.at[0])
         stage[:, :, 40:WEIGHT_ROWS, :] = jnp.zeros((2, 3, WEIGHT_ROWS - 40, D), BF16)
-        for half in range(2):
-            for m in range(3):
-                if half == 0:
-                    load(m).wait()
+        part = pl.ds(pl.multiple_of(y * 32, 32), 32)
+        all_core1(WQ, WQ, wq_h, wqb.at[0, part])
+        all_core1(WK, WK, wk_h, wkb.at[0, part])
+        all_core1(WV, WV, wv_h, wvb.at[0, part])
+        drain(WQ, wqb.at[0])
+        drain(WK, wkb.at[0])
+        drain(WV, wvb.at[0])
+        for m in range(3):
+            load(m).wait()
+
+        @pl.loop(0, 3)
+        def _(m):
+            for half in range(2):
                 stage[half, m, 0:hidden_rows, :] = raw.at[m][:, half, :]
-            for m in range(3):
                 send(W0 + half, W0 + half, stage.at[half, m], wts.at[half, m, pl.ds(WEIGHT_ROWS, WEIGHT_ROWS)], core1)
-            drain(W0 + half, stage.at[half])
-            if half == 0:
-                part = pl.ds(pl.multiple_of(y * 32, 32), 32)
-                all_core1(WQ, WQ, wq_h, wqb.at[0, part])
-                all_core1(WK, WK, wk_h, wkb.at[0, part])
-                all_core1(WV, WV, wv_h, wvb.at[0, part])
-                drain(WQ, wqb.at[0])
-                drain(WK, wkb.at[0])
-                drain(WV, wvb.at[0])
+
+        drain(W0, stage.at[0])
+        drain(W1, stage.at[1])
         all_core1(WO, WO, po_h, pob.at[part, pl.ds(0, 512)])
         drain(WO, pob.at[:, pl.ds(0, 512)])
+        give(KX, ck_h, kbuf)
+        give(VX, cv_h, vbuf)
 
         for k in (3, 4, 6, 8, 9):
             load(k).wait()
+        arrive(KX, kbuf.at[pl.ds(0, NY - 1)])
+        arrive(VX, vbuf.at[pl.ds(0, NY - 1)])
         arrive(C3, c3)
-        attend()
-        for k in Y_STEPS + (0,):
-            p = y_peer(k)
-            send(D1, D1, d1s.at[p], d1r.at[y * NC], {"kv_1": p, "tp": 1})
+        attend(c3[...])
+        send(D1, D1, d1s, d1r, core1)
         drain(D1, d1s)
         sent_all()
         arrive(FS, fs)
@@ -232,18 +248,10 @@
         load(5).wait()
         a1[y * NC + 1] = own_tile()
 
-        def relayout(half):
-            for m in range(3):
-                wts[half, m, 0:hidden_rows, :] = raw.at[m][:, half, :]
-
         pl.semaphore_wait(hello, 1)
 
         to_y(A1, a1.at[y * NC + 1], a1.at[y * NC + 1])
         drain(A1, a1.at[pl.ds(0, NY - 1)])
-        wts[:, :, 40:WEIGHT_ROWS, :] = jnp.zeros((2, 3, WEIGHT_ROWS - 40, D), BF16)
-        for m in range(3):
-            load(m).wait()
-        relayout(0)
         arrive(A1, a1.at[pl.ds(0, NYC - 1)])
         res_z = total(a1, NYC)
         a2[z] = res_z.astype(BF16)
@@ -258,9 +266,18 @@
         drain(WK, wkb.at[1, pl.ds(0, 96)])
         drain(WV, wvb.at[1, pl.ds(0, 96)])
         drain(WO, pob.at[pl.ds(0, 96), pl.ds(512, 512)])
+        give(KX, ck_h, kbuf)
         load(7).wait()
         lams[1] = own_lambdas()
-        relayout(1)
+        wts[:, :, 40:WEIGHT_ROWS, :] = jnp.zeros((2, 3, WEIGHT_ROWS - 40, D), BF16)
+        for m in range(3):
+            load(m).wait()
+
+        @pl.loop(0, 3)
+        def _(m):
+            for half in range(2):
+                wts[half, m, 0:hidden_rows, :] = raw.at[m][:, half, :]
+
         for k in (6, 8, 9):
             load(k).wait()
         for pull in pulls:
@@ -279,6 +296,7 @@
         b2[y] = total(b1r, NZ)
         to_y(B2, b2.at[y], b2.at[y])
         drain(B2, b2.at[pl.ds(0, NY - 1)])
+        give(VX, cv_h, vbuf)
         arrive(WQ, wqb.at[:, pl.ds(0, 112)])
         arrive(WK, wkb.at[:, pl.ds(0, 112)])
         arrive(WV, wvb.at[:, pl.ds(0, 112)])
@@ -290,14 +308,12 @@
         query = [jnp.dot(scaled, wqb[t], preferred_element_type=F32) for t in range(2)]
         squares = jnp.sum(stream_one * stream_one, axis=1, keepdims=True)
         csq[z] = jnp.sum(jnp.where(lane == row, squares, 0.0), axis=0, keepdims=True)
+        to_z(CQ, lambda p: csq.at[z], csq)
         for t in range(2):
             for g in range(4):
                 cs[pl.ds(t * 4 + g, 8, stride=8), :] = query[t][:, g * LANES : (g + 1) * LANES]
         pair = pl.ds(pl.multiple_of(y * 16, 16), 16)
-        for k in Z_STEPS:
-            p = z_peer(k)
-            send(CQ, CQ, csq.at[z], csq.at[z], {"kv_0": p})
-            send(C2, C2, cs.at[pair], c2.at[z], {"kv_0": p})
+        to_z(C2, lambda p: cs.at[pair], c2)
         drain(CQ, csq.at[pl.ds(0, NZ - 1)])
         drain(C2, c2.at[pl.ds(0, NZ - 1)])
         c2[z] = cs[pair, :]
@@ -331,22 +347,13 @@
             c3s[t] = jnp.concatenate(
                 [queries[t * 8 : t * 8 + 8], queries[16 + t * 8 : 24 + t * 8]], axis=0
             ).astype(BF16)
-        for k in Y_STEPS:
-            send(C3S, C3, c3s.at[0], c3.at[y], {"kv_1": y_peer(k), "tp": 0})
-            send(C3, C3, c3s.at[1], c3.at[y], {"kv_1": y_peer(k)})
-        send(C3S, C3, c3s.at[0], c3.at[y], {"tp": 0})
-        drain(C3S, c3)
-        drain(C3, c3.at[pl.ds(0, NY - 1)])
-        c3[y] = c3s[1]
+        send(C3, C3, c3s.at[0], c3, {"tp": 0})
+        drain(C3, c3)
         load(3).wait()
         load(4).wait()
-        arrive(C3, c3.at[pl.ds(0, NY - 1)])
-        attend()
-        for k in Y_STEPS:
-            p = y_peer(k)
-            send(D1, D1, d1s.at[p], d1r.at[y * NC + 1], {"kv_1": p})
-        drain(D1, d1s.at[pl.ds(0, NY - 1)])
-        d1r[y * NC + 1] = d1s[y]
+        arrive(KX, kbuf.at[pl.ds(0, NY - 1)])
+        arrive(VX, vbuf.at[pl.ds(0, NY - 1)])
+        attend(c3s[1])
 
         @pl.when(z == owner)
         def _():
@@ -377,13 +384,14 @@
         arrive(LAM, lams.at[0])
         arrive(WO, pob.at[pl.ds(0, 112)])
         arrive(W1, wts.at[1, :, pl.ds(WEIGHT_ROWS, WEIGHT_ROWS)])
-        arrive(D1, d1r.at[pl.ds(0, NYC - 1)])
+        arrive(D1, d1r)
 
         is_top = lax.rem(lane, HEAD) < HEAD // 2
         joined, line = [[], []], jnp.zeros((1, LANES), F32)
         for t in range(2):
-            stats = [d1r[k * NC + t, 16:24, :] for k in range(NY)] + [own[t]]
-            blocks = [[d1r[k * NC + t, s * 8 : s * 8 + 8, :] for s in range(2)] for k in range(NY)]
+            part = (d1r, d1s)[t]
+            stats = [part[k, 16:24, :] for k in range(NY)] + [own[t]]
+            blocks = [[part[k, s * 8 : s * 8 + 8, :] for s in range(2)] for k in range(NY)]
             blocks += [[own[2 + t], own[4 + t]]]
             top = functools.reduce(jnp.maximum, stats)
             weights = [jnp.where(is_top, jnp.exp(jnp.where(is_top, each - top, 0.0)), 0.0) for each in stats]
@@ -400,10 +408,8 @@
                 )
         d2m[z] = line
         d2o[z] = jnp.concatenate(joined[0] + joined[1], axis=0).astype(BF16)
-        for k in Z_STEPS:
-            p = z_peer(k)
-            send(D2M, D2M, d2m.at[z], d2m.at[z], {"kv_0": p})
-            send(D2O, D2O, d2o.at[z], d2o.at[z], {"kv_0": p})
+        to_z(D2M, lambda p: d2m.at[z], d2m)
+        to_z(D2O, lambda p: d2o.at[z], d2o)
         drain(D2M, d2m.at[pl.ds(0, NZ - 1)])
         drain(D2O, d2o.at[pl.ds(0, NZ - 1)])
         arrive(D2M, d2m.at[pl.ds(0, NZ - 1)])
@@ -466,10 +472,10 @@
         finish(stream_two)
 
 
-PHASES = 25
+PHASES = 26
 (
-    A1, A2, B1, B2, CQ, C2, CKV, C3, C3S, D1, D2O, D2M, D3, F2, FS, G1, G2, G2S, LAM, W0, W1, WQ, WK, WV, WO,
-) = range(25)
+    A1, A2, B1, B2, CQ, C2, CKV, C3, D1, D2O, D2M, D3, F2, FS, G1, G2, G2S, LAM, W0, W1, WQ, WK, WV, WO, KX, VX,
+) = range(26)
 
 
 def local(
@@ -500,8 +506,8 @@
             pltpu.VMEM((2, LANES, 128), BF16),
             pltpu.VMEM((LANES, 1024), BF16),
             pltpu.VMEM((2, 8, LANES), F32),
-            pltpu.VMEM((batch, span, 128), BF16),
-            pltpu.VMEM((batch, span, VDIM), BF16),
+            pltpu.VMEM((NY, batch // NY, span, 128), BF16),
+            pltpu.VMEM((NY, batch // NY, span, VDIM), BF16),
             pltpu.VMEM((NYC, 8, LANES), BF16),
             pltpu.VMEM((NZ, 8, LANES), BF16),
             pltpu.VMEM((NZ, 8, LANES), F32),
@@ -514,9 +520,9 @@
             pltpu.VMEM((NZ, 8, LANES), F32),
             pltpu.VMEM((6, 8, LANES), F32),
             pltpu.VMEM((2, 16, LANES), BF16),
-            pltpu.VMEM((NY, 16, LANES), BF16),
+            pltpu.VMEM((16, LANES), BF16),
             pltpu.VMEM((NY, 24, LANES), F32),
-            pltpu.VMEM((NYC, 24, LANES), F32),
+            pltpu.VMEM((NY, 24, LANES), F32),
             pltpu.VMEM((NZ, 32, LANES), BF16),
             pltpu.VMEM((NZ, 1, LANES), F32),
             pltpu.VMEM((32, LANES), F32),

time: 70.9 us -> 66.8 us (0.942)
  Pallas kernels: 70.1 us -> 66.1 us
    pallas_call x1, Pallas kernels: 70.1 us -> 66.1 us  [local(): pl.pallas_call(layer_kernel, out_shape=pltpu.VMEM(residual.shape, F32), i...]
where the time goes in v7:
time: 66.8 us; the launch traced here: 66.7 us
  Pallas kernels  66.1 us (99%)
    pallas_call x1, Pallas kernels, local(): pl.pallas_call(layer_kernel, out_shape=pltpu.VMEM(residual.shape, F32), i...  66.1 us

profile of v7, /device:TPU:1, one launch (start us, length us, event | category | flops | bytes accessed | tf_op | source)
XLA Modules:
  0.0 66.7 jit_solution(10502666624048066987)
XLA Ops:
  0.0 66.1 %shard_map.136 = f32[8,16]{1,0:T(8,128)S(1)} custom-call(bf16[8,16]{1,0:T(8,128)(2,1)} %res_h.1, f32[3,2048]{1,0:T(4,128)} %gains_h.1, bf16[44,2,2048]{2,1,0:T(2,128)(2,1)} %bitcast.9, bf16[44,2,2048]{2,1,0:T(2,128)(2,1)} %bitcast.10, bf16[44,2,2048]{2,1,0:T(2,128)(2,1)} %bitcast.11, bf16[32,512]{1,0:T(8,128)(2,1)} %wq_h.1, bf16[32,128]{1,0:T(8,128)(2,1)} %wk_h.1, ...), custom_call_target="tpu_custom_call" | custom-call | tf_op jit(solution)/shard_map/pallas_call | solution.py:490
  66.1 0.6 convert_element_type.3

commit v8 on v7

--- a/solution.py
+++ b/solution.py
@@ -47,7 +47,7 @@
     out,
     res, gains, lam, hgain, live,
     raw, stage, wts, wqb, wkb, wvb, pob, lams, kbuf, vbuf,
-    a1, a2, b1s, b1r, b2, cs, ckvs, csq, c2, ckv, own, c3s, c3, d1s, d1r, d2o, d2m, hs, d3s, d3, ps, f2, fs, g1s, g1r, g2,
+    a1, a2, b1s, b1r, b2, cs, ckvs, csq, c2, ckv, own, c3s, d1s, d2o, d2m, hs, d3s, d3, ps, f2, fs, g1s, g1r, g2,
     hsem, ssem, rsem, hello,
 ):
     z = lax.axis_index("kv_0")
@@ -105,10 +105,10 @@
         src = (ck_h, cv_h, res_h, gains_h, lam_h, hgain_h, live_h)[k - 3]
         if k < 5:
             src = src.at[pl.ds(2 * y, 2)]
-        return pltpu.make_async_copy(src, (kbuf.at[y], vbuf.at[y], res, gains, lam, hgain, live)[k - 3], hsem.at[k])
-
-    def start_loads():
-        for k in (5, 0, 1, 2, 7, 6, 8, 9, 3, 4):
+        return pltpu.make_async_copy(src, (kbuf.at[y * NC + 1], vbuf.at[y * NC + 1], res, gains, lam, hgain, live)[k - 3], hsem.at[k])
+
+    def start_loads(which):
+        for k in which:
             load(k).start()
 
     def own_tile():
@@ -122,43 +122,47 @@
         head = row // 2
         return jnp.where(head == 0, lam[0], jnp.where(head == 1, lam[1], jnp.where(head == 2, lam[2], lam[3])))
 
-    def attend(tile):
+    def attend():
         span = kbuf.shape[2]
-        queries = tile.astype(F32)
-        queries = [queries[t * 8 : t * 8 + 8].astype(BF16) for t in range(2)]
+        queries = [c3s[t].astype(F32) for t in range(NC)]
+        cases = [(t, k, s) for t in range(NC) for k in range(NY) for s in range(2)]
         scores = jnp.concatenate(
             [
-                lax.dot_general(queries[b % 2], kbuf[b // 2, b % 2], NT, preferred_element_type=F32)
-                for b in range(8)
+                lax.dot_general(
+                    queries[t][s * 8 : s * 8 + 8].astype(BF16), kbuf[k * NC + t, s], NT, preferred_element_type=F32
+                )
+                for t, k, s in cases
             ],
             axis=0,
         ) * HEAD**-0.5
         place = z * NY * span + iota((8, span), 1)
         length = [live[2 * y], live[2 * y + 1]]
-        alive = jnp.concatenate(
-            [(place + (b // 2) * span < length[b % 2]).astype(F32) for b in range(8)], axis=0
-        ) > 0.0
+        alive = jnp.concatenate([(place + k * span < length[s]).astype(F32) for t, k, s in cases], axis=0) > 0.0
         highest = jnp.max(jnp.where(alive, scores, -1e30), axis=1, keepdims=True)
         terms = jnp.where(alive, jnp.exp(scores - highest), 0.0)
         weights = terms.astype(BF16)
-        values = [jnp.dot(weights[b * 8 : b * 8 + 8], vbuf[b // 2, b % 2], preferred_element_type=F32) for b in range(8)]
+        values = [
+            jnp.dot(weights[b * 8 : b * 8 + 8], vbuf[k * NC + t, s], preferred_element_type=F32)
+            for b, (t, k, s) in enumerate(cases)
+        ]
         count = jnp.sum(terms, axis=1, keepdims=True)
-        for k in range(NY):
+        for b in range(0, len(cases), 2):
+            t, k, _ = cases[b]
             pairs = [
                 jnp.where(
-                    lax.rem(lane, HEAD) < HEAD // 2, highest[b * 8 : b * 8 + 8], count[b * 8 : b * 8 + 8]
+                    lax.rem(lane, HEAD) < HEAD // 2, highest[a * 8 : a * 8 + 8], count[a * 8 : a * 8 + 8]
                 )
-                for b in (2 * k, 2 * k + 1)
+                for a in (b, b + 1)
             ]
-            d1s[k, 0:8, :] = values[2 * k]
-            d1s[k, 8:16, :] = values[2 * k + 1]
-            d1s[k, 16:24, :] = jnp.where(lane < HEAD, pairs[0], pairs[1])
-
-    def give(phase, cache, buf):
-        for k in Y_STEPS:
+            d1s[t, k, 0:8, :] = values[b]
+            d1s[t, k, 8:16, :] = values[b + 1]
+            d1s[t, k, 16:24, :] = jnp.where(lane < HEAD, pairs[0], pairs[1])
+
+    def give(phase, cache, buf, steps):
+        for k in steps:
             p = y_peer(k)
-            send(phase, phase, cache.at[pl.ds(2 * p, 2)], buf.at[y], {"kv_1": p})
-        drain(phase, buf.at[pl.ds(0, NY - 1)])
+            send(phase, phase, cache.at[pl.ds(2 * p, 2)], buf.at[y * NC + c], {"kv_1": p, "tp": 1})
+        drain(phase, buf.at[pl.ds(0, len(steps))])
 
     def sent_all():
         for each in drains:
@@ -178,12 +182,10 @@
             for k in Y_STEPS + (0,):
                 send(s, r, src, dst, {"kv_1": y_peer(k), "tp": 1})
 
-        for k in Y_STEPS:
-            signal({"kv_1": y_peer(k)})
-        start_loads()
+        start_loads((5, 0, 1, 2, 7))
         load(5).wait()
         a1[y * NC] = own_tile()
-        pl.semaphore_wait(barrier, NY + NY - 1)
+        pl.semaphore_wait(barrier, NY)
         pl.semaphore_signal(hello, inc=1, device_id=core1, device_id_type=MESH)
 
         all_core1(A1, A1, a1.at[y * NC], a1.at[y * NC])
@@ -213,17 +215,9 @@
         drain(W1, stage.at[1])
         all_core1(WO, WO, po_h, pob.at[part, pl.ds(0, 512)])
         drain(WO, pob.at[:, pl.ds(0, 512)])
-        give(KX, ck_h, kbuf)
-        give(VX, cv_h, vbuf)
-
-        for k in (3, 4, 6, 8, 9):
-            load(k).wait()
-        arrive(KX, kbuf.at[pl.ds(0, NY - 1)])
-        arrive(VX, vbuf.at[pl.ds(0, NY - 1)])
-        arrive(C3, c3)
-        attend(c3[...])
-        send(D1, D1, d1s, d1r, core1)
-        drain(D1, d1s)
+        give(KX, ck_h, kbuf, Y_STEPS + (0,))
+        give(VX, cv_h, vbuf, Y_STEPS + (0,))
+
         sent_all()
         arrive(FS, fs)
         arrive(G2, g2)
@@ -235,7 +229,7 @@
             signal({"kv_0": z_peer(k)})
         for k in Y_STEPS + (0,):
             signal({"kv_1": y_peer(k), "tp": 0})
-        start_loads()
+        start_loads((5, 0, 1, 2, 7, 6, 8, 9, 3, 4))
         part = pl.ds(pl.multiple_of(y * 32, 32), 32)
         pulls = [
             pltpu.make_async_copy(wq_h, wqb.at[1, part], hsem.at[10]),
@@ -266,7 +260,7 @@
         drain(WK, wkb.at[1, pl.ds(0, 96)])
         drain(WV, wvb.at[1, pl.ds(0, 96)])
         drain(WO, pob.at[pl.ds(0, 96), pl.ds(512, 512)])
-        give(KX, ck_h, kbuf)
+        give(KX, ck_h, kbuf, Y_STEPS)
         load(7).wait()
         lams[1] = own_lambdas()
         wts[:, :, 40:WEIGHT_ROWS, :] = jnp.zeros((2, 3, WEIGHT_ROWS - 40, D), BF16)
@@ -296,7 +290,7 @@
         b2[y] = total(b1r, NZ)
         to_y(B2, b2.at[y], b2.at[y])
         drain(B2, b2.at[pl.ds(0, NY - 1)])
-        give(VX, cv_h, vbuf)
+        give(VX, cv_h, vbuf, Y_STEPS)
         arrive(WQ, wqb.at[:, pl.ds(0, 112)])
         arrive(WK, wkb.at[:, pl.ds(0, 112)])
         arrive(WV, wvb.at[:, pl.ds(0, 112)])
@@ -347,13 +341,11 @@
             c3s[t] = jnp.concatenate(
                 [queries[t * 8 : t * 8 + 8], queries[16 + t * 8 : 24 + t * 8]], axis=0
             ).astype(BF16)
-        send(C3, C3, c3s.at[0], c3, {"tp": 0})
-        drain(C3, c3)
         load(3).wait()
         load(4).wait()
-        arrive(KX, kbuf.at[pl.ds(0, NY - 1)])
-        arrive(VX, vbuf.at[pl.ds(0, NY - 1)])
-        attend(c3s[1])
+        arrive(KX, kbuf.at[pl.ds(0, NYC - 1)])
+        arrive(VX, vbuf.at[pl.ds(0, NYC - 1)])
+        attend()
 
         @pl.when(z == owner)
         def _():
@@ -384,14 +376,12 @@
         arrive(LAM, lams.at[0])
         arrive(WO, pob.at[pl.ds(0, 112)])
         arrive(W1, wts.at[1, :, pl.ds(WEIGHT_ROWS, WEIGHT_ROWS)])
-        arrive(D1, d1r)
 
         is_top = lax.rem(lane, HEAD) < HEAD // 2
         joined, line = [[], []], jnp.zeros((1, LANES), F32)
         for t in range(2):
-            part = (d1r, d1s)[t]
-            stats = [part[k, 16:24, :] for k in range(NY)] + [own[t]]
-            blocks = [[part[k, s * 8 : s * 8 + 8, :] for s in range(2)] for k in range(NY)]
+            stats = [d1s[t, k, 16:24, :] for k in range(NY)] + [own[t]]
+            blocks = [[d1s[t, k, s * 8 : s * 8 + 8, :] for s in range(2)] for k in range(NY)]
             blocks += [[own[2 + t], own[4 + t]]]
             top = functools.reduce(jnp.maximum, stats)
             weights = [jnp.where(is_top, jnp.exp(jnp.where(is_top, each - top, 0.0)), 0.0) for each in stats]
@@ -472,10 +462,10 @@
         finish(stream_two)
 
 
-PHASES = 26
+PHASES = 24
 (
-    A1, A2, B1, B2, CQ, C2, CKV, C3, D1, D2O, D2M, D3, F2, FS, G1, G2, G2S, LAM, W0, W1, WQ, WK, WV, WO, KX, VX,
-) = range(26)
+    A1, A2, B1, B2, CQ, C2, CKV, D2O, D2M, D3, F2, FS, G1, G2, G2S, LAM, W0, W1, WQ, WK, WV, WO, KX, VX,
+) = range(24)
 
 
 def local(
@@ -506,8 +496,8 @@
             pltpu.VMEM((2, LANES, 128), BF16),
             pltpu.VMEM((LANES, 1024), BF16),
             pltpu.VMEM((2, 8, LANES), F32),
-            pltpu.VMEM((NY, batch // NY, span, 128), BF16),
-            pltpu.VMEM((NY, batch // NY, span, VDIM), BF16),
+            pltpu.VMEM((NYC, batch // NY, span, 128), BF16),
+            pltpu.VMEM((NYC, batch // NY, span, VDIM), BF16),
             pltpu.VMEM((NYC, 8, LANES), BF16),
             pltpu.VMEM((NZ, 8, LANES), BF16),
             pltpu.VMEM((NZ, 8, LANES), F32),
@@ -520,9 +510,7 @@
             pltpu.VMEM((NZ, 8, LANES), F32),
             pltpu.VMEM((6, 8, LANES), F32),
             pltpu.VMEM((2, 16, LANES), BF16),
-            pltpu.VMEM((16, LANES), BF16),
-            pltpu.VMEM((NY, 24, LANES), F32),
-            pltpu.VMEM((NY, 24, LANES), F32),
+            pltpu.VMEM((NC, NY, 24, LANES), F32),
             pltpu.VMEM((NZ, 32, LANES), BF16),
             pltpu.VMEM((NZ, 1, LANES), F32),
             pltpu.VMEM((32, LANES), F32),

time: 66.8 us -> 65.8 us (0.985)
  Pallas kernels: 66.1 us -> 65.1 us
    pallas_call x1, Pallas kernels: 66.1 us -> 65.1 us  [local(): pl.pallas_call(layer_kernel, out_shape=pltpu.VMEM(residual.shape, F32), i...]
where the time goes in v8:
time: 65.8 us; the launch traced here: 65.7 us
  Pallas kernels  65.1 us (99%)
    pallas_call x1, Pallas kernels, local(): pl.pallas_call(layer_kernel, out_shape=pltpu.VMEM(residual.shape, F32), i...  65.1 us

profile of v8, /device:TPU:1, one launch (start us, length us, event | category | flops | bytes accessed | tf_op | source)
XLA Modules:
  0.0 65.7 jit_solution(14480578804444598543)
XLA Ops:
  0.0 65.1 %shard_map.136 = f32[8,16]{1,0:T(8,128)S(1)} custom-call(bf16[8,16]{1,0:T(8,128)(2,1)} %res_h.1, f32[3,2048]{1,0:T(4,128)} %gains_h.1, bf16[44,2,2048]{2,1,0:T(2,128)(2,1)} %bitcast.9, bf16[44,2,2048]{2,1,0:T(2,128)(2,1)} %bitcast.10, bf16[44,2,2048]{2,1,0:T(2,128)(2,1)} %bitcast.11, bf16[32,512]{1,0:T(8,128)(2,1)} %wq_h.1, bf16[32,128]{1,0:T(8,128)(2,1)} %wk_h.1, ...), custom_call_target="tpu_custom_call" | custom-call | tf_op jit(solution)/shard_map/pallas_call | solution.py:480
  65.1 0.6 convert_element_type.3
